TPU v7x, 256 devices: a whole 4x4x8 slice. The times are simulated.
256 devices in a mesh: ep: 128 (over z, y, x), tp: 2 (over core).
Axes of the slice: x: 4, y: 4, z: 8, core: 2. Of those that a mesh axis runs over, the one named last changes fastest.
Arguments:
- resid: bfloat16 [2048, 2048], P('ep'), may hold values from -6 to 6
- proj_x: bfloat16 [2048, 2048], P('ep', 'tp'), may hold values from -6 to 6
- proj_z: bfloat16 [2048, 2048], P('ep', 'tp'), may hold values from -6 to 6
- proj_bc: bfloat16 [2048, 2, 512], P('ep', None, 'tp'), may hold values from -6 to 6
- proj_dt: bfloat16 [2048, 32], P('ep', 'tp'), may hold values from -6 to 6
- tail_x: bfloat16 [2048, 3, 2048], P('ep', None, 'tp'), may hold values from -6 to 6
- tail_bc: bfloat16 [2048, 3, 2, 512], P('ep', None, None, 'tp'), may hold values from -6 to 6
- taps_x: bfloat16 [4, 2048], P(None, 'tp'), may hold values from -3 to 3
- taps_bc: bfloat16 [4, 2, 512], P(None, None, 'tp'), may hold values from -3 to 3
- ssm_state: float32 [2048, 32, 4096], P('ep', 'tp'), may hold values from -1.5 to 1.5
- dt_bias: float32 [32], P('tp'), may hold values from -4 to 0
- decay_log: float32 [32], P('tp'), may hold values from -1 to 2.5
- group_gain: float32 [2048], P('tp'), may hold values from 0.1 to 1.9
- out_proj: bfloat16 [2048, 2048], P('tp', 'ep'), may hold values from -0.125 to 0.125
- ffn_gain: float32 [2048], replicated, may hold values from 0.1 to 1.9
- dense_gate: bfloat16 [2048, 4096], P(None, ('ep', 'tp')), may hold values from -0.125 to 0.125
- dense_up: bfloat16 [2048, 4096], P(None, ('ep', 'tp')), may hold values from -0.125 to 0.125
- dense_down: bfloat16 [4096, 2048], P(('ep', 'tp')), may hold values from -0.09375 to 0.09375
- branch_gate: bfloat16 [2048], replicated, may hold values from -0.125 to 0.125
- group_weights: float32 [2048, 4], replicated, may hold values from 0.2 to 1
- expert_ids: int32 [2048, 6], replicated, may hold values from 0 to 127, all different within a row; in each aligned block of 16 rows (0 to 15, 16 to 31, ...) at most 2 rows name the same one
- expert_weights: float32 [2048, 6], replicated, may hold values from 0.1 to 1
- exp_gate: bfloat16 [128, 2048, 512], P('ep', None, 'tp'), may hold values from -0.125 to 0.125
- exp_up: bfloat16 [128, 2048, 512], P('ep', None, 'tp'), may hold values from -0.125 to 0.125
- exp_down: bfloat16 [128, 512, 2048], P('ep', 'tp'), may hold values from -0.25 to 0.25
Outputs:
- out: bfloat16 [2048, 2048], P(('ep', 'tp'))
- new_state: float32 [2048, 32, 4096], P('ep', 'tp')
Inputs may be any that keep to these rules, and one draw needn't show every extreme that they name: `expert_ids`: each row names 6 different experts. In the rows of one index of ep (aligned blocks of 16 rows) no expert is named more than 2 times, a bound that some block reaches.
All inputs are finite; a program needn't handle non-finite values.
Results may differ from a plain program's by a relative error of at most 0.013.
Values may be sent and summed in bfloat16 or wider, within the bound.
A program may use at most 128 MiB of HBM per device.

v0:
```python
import jax
import jax.numpy as jnp
from jax import lax
from jax.sharding import Mesh
from jax.sharding import PartitionSpec as P

HEAD_P = 64
NSTATE = 64
GROUPS = 4
TOPK = 6
HPG = 4
EP = ("ep_0", "ep_1", "ep_2")
EP_TP = ("ep_0", "ep_1", "ep_2", "tp")


EPSILON = 1e-06


def gathered_by_axis(shard, axes, dim):
    if not axes:
        return shard
    nearer = lax.all_gather(shard, axes[-1], axis=dim, tiled=True)
    return gathered_by_axis(nearer, axes[:-1], dim)


def sent_to_all(shard, axis):
    copies = jnp.broadcast_to(shard, (lax.axis_size(axis), *shard.shape))
    return lax.all_to_all(copies, axis, split_axis=0, concat_axis=0, tiled=True)


def of_everyone(shard, axis):
    everything = sent_to_all(shard, axis)
    return jnp.sum(everything.astype(jnp.float32), axis=0)


def split_up(shard, dim, devices):
    before, after = (shard.shape[:dim], shard.shape[dim + 1 :])
    return jnp.moveaxis(shard.reshape(*before, devices, -1, *after), dim, 0)


def sum_at_owner(shard, axis, dim):
    devices = lax.axis_size(axis)
    pieces = lax.all_to_all(split_up(shard, dim, devices), axis, 0, 0, tiled=True)
    return jnp.sum(pieces.astype(jnp.float32), axis=0)


def summed_rows(shard, axes, dim):
    far, near = axes
    pieces = split_up(shard, dim, lax.axis_size(far))
    nearer = sum_at_owner(pieces, near, dim + 1)
    arrived = lax.all_to_all(
        nearer.astype(jnp.bfloat16), far, split_axis=0, concat_axis=0, tiled=True
    )
    return arrived.astype(jnp.float32).sum(axis=0)


def state_update(
    proj_x,
    proj_z,
    proj_bc,
    proj_dt,
    tail_x,
    tail_bc,
    taps_x,
    taps_bc,
    ssm_state,
    dt_bias,
    decay_log,
    group_gain,
):
    window_x = jnp.concatenate([tail_x, proj_x[:, None]], axis=1).astype(jnp.float32)
    conv_x = jax.nn.silu(jnp.sum(window_x * taps_x.astype(jnp.float32)[None], axis=1))
    window_bc = jnp.concatenate([tail_bc, proj_bc[:, None]], axis=1).astype(jnp.float32)
    conv_bc = jax.nn.silu(jnp.sum(window_bc * taps_bc.astype(jnp.float32)[None], axis=1))
    count = proj_x.shape[0]
    heads = proj_dt.shape[1]
    x_heads = conv_x.reshape(count, heads, HEAD_P)
    grouped_bc = conv_bc.reshape(count, 2, heads // HPG, NSTATE)
    input_heads = jnp.repeat(grouped_bc[:, 0], HPG, axis=1)
    read_heads = jnp.repeat(grouped_bc[:, 1], HPG, axis=1)
    step_size = jax.nn.softplus(proj_dt.astype(jnp.float32) + dt_bias)
    decay = jnp.exp(-step_size * jnp.exp(decay_log))
    state = ssm_state.reshape(count, heads, HEAD_P, NSTATE)
    fresh = (step_size[:, :, None] * x_heads)[:, :, :, None] * input_heads[:, :, None, :]
    new_state = decay[:, :, None, None] * state + fresh
    readout = jnp.sum(new_state * read_heads[:, :, None, :], axis=-1)
    gated = readout.reshape(count, heads * HEAD_P) * jax.nn.silu(proj_z.astype(jnp.float32))
    grouped = gated.reshape(count, heads // HPG, HPG * HEAD_P)
    grouped = grouped * lax.rsqrt(jnp.mean(grouped * grouped, axis=-1, keepdims=True) + EPSILON)
    y_out = (grouped.reshape(count, heads * HEAD_P) * group_gain).astype(jnp.bfloat16)
    return (y_out, new_state.reshape(count, heads, HEAD_P * NSTATE))


def shards(
    resid,
    proj_x,
    proj_z,
    proj_bc,
    proj_dt,
    tail_x,
    tail_bc,
    taps_x,
    taps_bc,
    ssm_state,
    dt_bias,
    decay_log,
    group_gain,
    out_proj,
    ffn_gain,
    dense_gate,
    dense_up,
    dense_down,
    branch_gate,
    group_weights,
    expert_ids,
    expert_weights,
    exp_gate,
    exp_up,
    exp_down,
):
    y_out, new_state = state_update(
        proj_x,
        proj_z,
        proj_bc,
        proj_dt,
        tail_x,
        tail_bc,
        taps_x,
        taps_bc,
        ssm_state,
        dt_bias,
        decay_log,
        group_gain,
    )
    partial_value = jnp.dot(
        y_out, gathered_by_axis(out_proj, EP, 1), preferred_element_type=jnp.float32
    )
    mixed = of_everyone(partial_value.astype(jnp.bfloat16), "tp").astype(jnp.float32)
    resid_new = (resid.astype(jnp.float32) + mixed).astype(jnp.bfloat16)
    widened = resid_new.astype(jnp.float32)
    normed = (
        widened
        * lax.rsqrt(jnp.mean(widened * widened, axis=-1, keepdims=True) + EPSILON)
        * ffn_gain
    ).astype(jnp.bfloat16)
    gathered = lax.all_gather(normed, EP, axis=0, tiled=True)
    score = jnp.dot(gathered, branch_gate, preferred_element_type=jnp.float32)
    dense_pre = jnp.dot(gathered, dense_gate, preferred_element_type=jnp.float32)
    dense_lin = jnp.dot(gathered, dense_up, preferred_element_type=jnp.float32)
    dense_hidden = (jax.nn.sigmoid(score)[:, None] * jax.nn.silu(dense_pre) * dense_lin).astype(
        jnp.bfloat16
    )
    experts = lax.axis_size(EP)
    expert_own = lax.axis_index(EP)
    cores = lax.axis_size("tp")
    core_index = lax.axis_index("tp")
    batch = gathered.shape[0]
    rows_each = batch // experts
    half_rows = rows_each // cores
    pairs = rows_each * TOPK
    capacity = (pairs + experts - 1) // experts + 1
    group_size = experts // GROUPS
    levels = jnp.arange(1, capacity + 1, dtype=jnp.int32)
    pair_row = jnp.arange(pairs, dtype=jnp.int32) // TOPK
    pick = (jnp.arange(GROUPS, dtype=jnp.int32) == expert_own // group_size).astype(jnp.float32)
    coarse = jnp.sum(group_weights * pick[None], axis=1)
    pair_weight = (expert_weights * coarse[:, None]).reshape(experts, pairs)
    hits = (expert_ids.reshape(experts, pairs) == expert_own).astype(jnp.int32)
    ranks = jnp.cumsum(hits, axis=1, dtype=jnp.int32)
    select = hits[:, None, :] * (ranks[:, None, :] == levels[None, :, None]).astype(jnp.int32)
    local_row = jnp.sum(select * pair_row[None, None, :], axis=-1, dtype=jnp.int32)
    filled = jnp.sum(select, axis=-1, dtype=jnp.int32).reshape(-1)
    slot_weight = jnp.sum(select.astype(jnp.float32) * pair_weight[:, None, :], axis=-1).reshape(-1)
    row_index = (local_row + jnp.arange(experts, dtype=jnp.int32)[:, None] * rows_each).reshape(-1)
    slot_rows = jnp.take(gathered, row_index, axis=0)
    slot_pre = jnp.dot(slot_rows, exp_gate[0], preferred_element_type=jnp.float32)
    slot_lin = jnp.dot(slot_rows, exp_up[0], preferred_element_type=jnp.float32)
    slot_hidden = (slot_weight[:, None] * jax.nn.silu(slot_pre) * slot_lin).astype(jnp.bfloat16)
    placing = (jnp.arange(batch, dtype=jnp.int32)[:, None] == row_index[None, :]) & (
        filled[None, :] > 0
    )
    row_hidden = jnp.dot(
        placing.astype(jnp.bfloat16), slot_hidden, preferred_element_type=jnp.float32
    ).astype(jnp.bfloat16)
    joined = jnp.concatenate([dense_hidden, row_hidden], axis=1)
    down_all = jnp.concatenate([dense_down, exp_down[0]], axis=0)
    inner_width = joined.shape[1]
    ordered = (
        joined.reshape(experts, cores, half_rows, inner_width)
        .transpose(1, 0, 2, 3)
        .reshape(batch, inner_width)
    )
    halved = sum_at_owner(
        jnp.dot(ordered, down_all, preferred_element_type=jnp.float32).astype(jnp.bfloat16), "tp", 0
    )
    branch = summed_rows(halved.astype(jnp.bfloat16), ("ep_0", ("ep_1", "ep_2")), 0)
    own_rows = lax.dynamic_slice_in_dim(widened, core_index * half_rows, half_rows, 0)
    out = (own_rows + branch).astype(jnp.bfloat16)
    return (out, new_state)


def solution(mesh):
    finer = Mesh(mesh.devices.reshape(8, 4, 4, mesh.shape["tp"]), ("ep_0", "ep_1", "ep_2", "tp"))
    in_specs = (
        P(EP, None),
        P(EP, "tp"),
        P(EP, "tp"),
        P(EP, None, "tp"),
        P(EP, "tp"),
        P(EP, None, "tp"),
        P(EP, None, None, "tp"),
        P(None, "tp"),
        P(None, None, "tp"),
        P(EP, "tp", None),
        P("tp"),
        P("tp"),
        P("tp"),
        P("tp", EP),
        P(),
        P(None, EP_TP),
        P(None, EP_TP),
        P(EP_TP, None),
        P(),
        P(),
        P(),
        P(),
        P(EP, None, "tp"),
        P(EP, None, "tp"),
        P(EP, "tp", None),
    )
    out_specs = (P(EP_TP, None), P(EP, "tp", None))
    return jax.shard_map(
        shards, mesh=finer, in_specs=in_specs, out_specs=out_specs, check_vma=False
    )
```

profile of v0, /device:TPU:1, one launch (start us, length us, event | category | flops | bytes accessed | tf_op | source)
XLA Modules:
  0.0 377.2 jit_solution(146625243671493132)
XLA Ops:
  7.2 10.6 %all_gather.12 = bf16[1024,64]{0,1:T(8,128)(2,1)S(1)} all-gather(bf16[1024,16]{0,1:T(8,128)(2,1)} %param.38), channel_id=1, replica_groups=mesh['ep_0'=8,'ep_1'=4,'ep_2'=4,'tp'=2] {'ep_2'}, dimensions={1}, use_global_device_ids=true | all-gather | bytes 163840 | tf_op jit(solution)/shard_map/all_gather | solution.py:22
  17.9 11.1 %all_gather.13 = bf16[1024,256]{0,1:T(8,128)(2,1)} all-gather(bf16[1024,64]{0,1:T(8,128)(2,1)S(1)} %all_gather.12), channel_id=1, replica_groups=mesh['ep_0'=8,'ep_1'=4,'ep_2'=4,'tp'=2] {'ep_1'}, dimensions={1}, use_global_device_ids=true | all-gather | bytes 655360 | tf_op jit(solution)/shard_map/all_gather | solution.py:22
  29.1 0.7 exp.39
  29.7 0.7 convert_element_type.92
  30.4 0.7 convert_element_type.90
  31.1 0.9 multiply_reduce_fusion.3
  32.1 0.1 reduce_sum.130
  32.2 0.9 multiply_reduce_fusion.1
  33.2 7.9 %reshape.179 = f32[16,16,64,64]{3,2,1,0:T(8,128)} reshape(f32[16,16,4096]{2,1,0:T(8,128)} %param.34) | data formatting | bytes 8388608 | tf_op jit(solution)/shard_map/reshape | solution.py:83
  41.4 8.4 %broadcast_multiply_fusion = (f32[16,16,64,64]{3,2,1,0:T(8,128)}, f32[16,16,64]{2,1,0:T(8,128)S(1)}) fusion(f32[16,16,64]{2,1,0:T(8,128)S(1)} %bitcast.42, f32[16,16,64]{2,1,0:T(8,128)S(1)} %multiply_multiply_fusion, f32[16,16,64]{2,1,0:T(8,128)S(1)} %bitcast.43, f32[16,16,64,64]{3,2,1,0:T(8,128)} %reshape.179, f32[16,16]{1,0:T(8,128)S(1)} %get-tuple-element.11), kind=kLoop, calls=%fused_computation.4 | loop fusion | flops 5226496 | bytes 8651776 | tf_op jit(solution)/shard_map/mul | solution.py:84
  50.2 41.0 %all-gather.3.cloned.1.call-done = bf16[1024,2048]{0,1:T(8,128)(2,1)} async-done(((bf16[1024,256]{0,1:T(8,128)(2,1)}), bf16[1024,2048]{0,1:T(8,128)(2,1)}) %all-gather.3.cloned.1.call-update) | async-done | bytes 4194320 | tf_op jit(solution)/shard_map/all_gather | solution.py:22
  91.2 3.4 convolution_convert_fusion.2
  94.6 4.4 %all_to_all.20 = bf16[2,16,2048]{2,1,0:T(8,128)(2,1)S(1)} all-to-all(bf16[2,16,2048]{2,1,0:T(8,128)(2,1)S(1)} %broadcast_in_dim.21), channel_id=1, replica_groups=mesh['ep_0'=8,'ep_1'=4,'ep_2'=4,'tp'=2] {'tp'}, dimensions={0} | all-to-all | bytes 262144 | tf_op jit(solution)/shard_map/all_to_all | solution.py:28
  99.0 0.1 multiply_reduce_fusion.2
  99.2 0.7 multiply_convert_fusion
  100.0 0.4 copy.48
  100.3 0.5 reshape.184
  100.9 0.1 reduce_window_sum.11
  101.3 0.1 add.161
  101.5 0.1 add.164
  101.6 0.1 copy.52
  101.8 0.1 gt.18
  102.1 0.4 copy.53
  102.5 0.5 mul.286
  103.2 0.1 copy.55
  103.3 0.1 mul.289
  103.5 115.4 %all-gather.5.cloned.1.call-done = bf16[2048,2048]{1,0:T(8,128)(2,1)} async-done(((bf16[16,2048]{1,0:T(8,128)(2,1)}), bf16[2048,2048]{1,0:T(8,128)(2,1)}) %all-gather.5.cloned.1.call-update) | async-done | bytes 8388624 | tf_op jit(solution)/shard_map/all_gather | solution.py:146
  218.9 5.6 %fusion.38 = f32[1,2048]{1,0:T(1,128)S(1)} fusion(bf16[2048,2048]{1,0:T(8,128)(2,1)} %all-gather.5.cloned.1.call-done, bf16[2048,1]{0,1:T(2,128)(2,1)S(1)} %reshape.193), kind=kOutput, calls=%fused_computation.84 | convolution fusion | flops 8388608 | bytes 8400896 | tf_op jit(solution)/shard_map/dot_general | solution.py:147
  224.6 6.8 %gather_fusion = bf16[256,2048]{1,0:T(8,128)(2,1)S(1)} fusion(bf16[2048,2048]{1,0:T(8,128)(2,1)} %all-gather.5.cloned.1.call-done, s32[1024]{0:T(1024)S(1)} %pad_clamp_fusion), kind=kCustom, calls=%fused_computation | custom fusion | bytes 2098176 | tf_op jit(solution)/shard_map/jit(_take)/gather | solution.py:175
  231.4 2.5 fusion.9
  233.9 2.4 convolution_convert_fusion.1
  236.3 5.7 %fusion.39 = f32[2048,16]{0,1:T(8,128)S(1)} fusion(bf16[2048,2048]{1,0:T(8,128)(2,1)} %all-gather.5.cloned.1.call-done, bf16[2048,16]{0,1:T(8,128)(2,1)S(1)} %copy-done.3), kind=kOutput, calls=%fused_computation.85 | convolution fusion | flops 134217728 | bytes 8585216 | tf_op jit(solution)/shard_map/dot_general | solution.py:148
  241.9 5.7 %fusion = bf16[2048,16]{0,1:T(8,128)(2,1)S(1)} fusion(bf16[2048,2048]{1,0:T(8,128)(2,1)} %all-gather.5.cloned.1.call-done, bf16[2048,16]{0,1:T(8,128)(2,1)S(1)} %copy-done.7, f32[2048,16]{0,1:T(8,128)S(1)} %fusion.39, f32[2048]{0:T(1024)S(1)} %add_divide_fusion), kind=kOutput, calls=%fused_computation.8 | convolution fusion | flops 134447104 | bytes 8658944 | tf_op jit(solution)/shard_map/dot_general | solution.py:149
  247.6 1.1 pad_maximum_fusion
  248.7 1.9 copy.57
  250.6 0.2 copy.58
  250.8 4.7 %convolution_convert_fusion = bf16[2048,2048]{1,0:T(8,128)(2,1)S(1)} fusion(bf16[2048,272]{1,0:T(8,128)(2,1)S(1)} %bitcast.41, bf16[256,2048]{1,0:T(8,128)(2,1)S(1)} %bitcast.50, bf16[16,2048]{1,0:T(8,128)(2,1)S(1)} %copy-done.15), kind=kOutput, calls=%fused_computation.2 | convolution fusion | flops 2288123904 | bytes 10616832 | tf_op jit(solution)/shard_map/dot_general | solution.py:194
  255.5 15.6 %all_to_all.21 = bf16[2,1024,2048]{2,1,0:T(8,128)(2,1)} all-to-all(bf16[2,1024,2048]{2,1,0:T(8,128)(2,1)S(1)} %bitcast.39), channel_id=1, replica_groups=mesh['ep_0'=8,'ep_1'=4,'ep_2'=4,'tp'=2] {'tp'}, dimensions={0} | all-to-all | bytes 16777216 | tf_op jit(solution)/shard_map/all_to_all | solution.py:43
  271.1 8.8 %reduce_sum.139 = bf16[1024,2048]{1,0:T(8,128)(2,1)} reduce(bf16[2,1024,2048]{2,1,0:T(8,128)(2,1)} %all_to_all.21, bf16[]{:T(256)} %constant.95.clone.1), dimensions={0}, to_apply=%region_11.12 | reduce | flops 2097152 | bytes 12582914 | tf_op jit(solution)/shard_map/reduce_sum | solution.py:44
  279.9 4.7 %copy.59 = bf16[16,8,8,2048]{3,2,1,0:T(8,128)(2,1)} copy(bf16[16,8,8,2048]{3,2,0,1:T(8,128)(2,1)} %bitcast.38) | data formatting | bytes 8388608 | tf_op jit(solution)/shard_map/transpose | solution.py:38
  284.6 5.0 %all-to-all-start.2 = ((bf16[16,8,8,2048]{3,2,1,0:T(8,128)(2,1)}), bf16[16,8,8,2048]{3,2,1,0:T(8,128)(2,1)}, u32[]{:S(2)}, u32[]{:S(2)}) async-start(bf16[16,8,8,2048]{3,2,1,0:T(8,128)(2,1)} %copy.59), calls=%async_computation.2 | async-start | bytes 8388608 | tf_op jit(solution)/shard_map/all_to_all | solution.py:43
  289.6 7.9 %mul.296 = f32[16,16,4096]{2,1,0:T(8,128)} reshape(f32[16,16,64,64]{3,2,1,0:T(8,128)} %get-tuple-element.6) | data formatting | bytes 8388608 | tf_op jit(solution)/shard_map/mul | solution.py:84
  297.5 54.9 %all-to-all-done.2 = bf16[16,8,8,2048]{3,2,1,0:T(8,128)(2,1)} async-done(((bf16[16,8,8,2048]{3,2,1,0:T(8,128)(2,1)}), bf16[16,8,8,2048]{3,2,1,0:T(8,128)(2,1)}, u32[]{:S(2)}, u32[]{:S(2)}) %all-to-all-start.2) | async-done | bytes 4194336 | tf_op jit(solution)/shard_map/all_to_all | solution.py:43
  352.4 3.7 reduce_sum.140
  356.1 3.9 %all-to-all-start.3 = ((bf16[8,8,2048]{2,1,0:T(8,128)(2,1)}), bf16[8,8,2048]{2,1,0:T(8,128)(2,1)S(1)}, u32[]{:S(2)}, u32[]{:S(2)}) async-start(bf16[8,8,2048]{2,1,0:T(8,128)(2,1)} %reduce_sum.140), calls=%async_computation.3 | async-start | bytes 524288 | tf_op jit(solution)/shard_map/all_to_all | solution.py:51
  360.0 6.6 %multiply_add_fusion = f32[16,16,4096]{2,1,0:T(8,128)} fusion(f32[16,16,4096]{2,1,0:T(8,128)} %mul.296, f32[16,16,4096]{2,1,0:T(8,128)} %param.34, f32[16,16]{1,0:T(8,128)S(1)} %get-tuple-element.11), kind=kLoop, calls=%fused_computation.3 | loop fusion | flops 2097152 | bytes 12583936 | tf_op jit(solution)/shard_map/add | solution.py:85
  366.6 3.1 all-to-all-done.3
  369.7 0.6 add_convert_fusion.1
  (73 shorter events, 1.6 us)
Async XLA Ops:
  7.2 226.7 %copy-start = (bf16[1,2048,256]{2,1,0:T(8,128)(2,1)S(1)}, bf16[1,2048,256]{2,1,0:T(8,128)(2,1)}, u32[]{:S(2)}) copy-start(bf16[1,2048,256]{2,1,0:T(8,128)(2,1)} %param.48) | copy-start | bytes 3145732
  7.2 84.0 %all-gather.3.cloned.1.call-start = ((), (), s32[]{:S(2)}) async-start(), calls=%async_computation.4 | async-start | bytes 4718592 | tf_op jit(solution)/shard_map/all_gather | solution.py:22
  29.0 189.9 %all-gather.5.cloned.1.call-start = ((), (), s32[]{:S(2)}) async-start(), calls=%async_computation.5 | async-start | bytes 8454144 | tf_op jit(solution)/shard_map/all_gather | solution.py:146
  33.2 7.9 %copy-start.12 = (bf16[16,16]{1,0:T(8,128)(2,1)S(1)}, bf16[16,16]{1,0:T(8,128)(2,1)}, u32[]{:S(2)}) copy-start(bf16[16,16]{1,0:T(8,128)(2,1)} %param.29) | copy-start | bytes 1540
  33.2 7.9 %copy-start.13 = (f32[16]{0:T(128)S(1)}, f32[16]{0:T(128)}, u32[]{:S(2)}) copy-start(f32[16]{0:T(128)} %param.35) | copy-start | bytes 196
  41.4 8.5 %copy-start.2 = (bf16[16,1024]{1,0:T(8,128)(2,1)S(1)}, bf16[16,1024]{1,0:T(8,128)(2,1)}, u32[]{:S(2)}) copy-start(bf16[16,1024]{1,0:T(8,128)(2,1)} %param.27) | copy-start | bytes 98308
  41.4 49.8 %copy-start.10 = (f32[1024]{0:T(1024)S(1)}, f32[1024]{0:T(1024)}, u32[]{:S(2)}) copy-start(f32[1024]{0:T(1024)} %param.37) | copy-start | bytes 12292
  49.8 49.2 %copy-start.4 = (bf16[16,2048]{1,0:T(8,128)(2,1)S(1)}, bf16[16,2048]{1,0:T(8,128)(2,1)}, u32[]{:S(2)}) copy-start(bf16[16,2048]{1,0:T(8,128)(2,1)} %param.25) | copy-start | bytes 196612
  49.8 49.4 %copy-start.9 = (f32[2048]{0:T(1024)S(1)}, f32[2048]{0:T(1024)}, u32[]{:S(2)}) copy-start(f32[2048]{0:T(1024)} %param.39) | copy-start | bytes 24580
  49.8 50.1 %copy-start.5 = (s32[2048,6]{0,1:T(8,128)S(1)}, s32[2048,6]{0,1:T(8,128)}, u32[]{:S(2)}) copy-start(s32[2048,6]{0,1:T(8,128)} %param.45) | copy-start | bytes 147460
  91.2 10.4 %copy-start.11 = (bf16[2048]{0:T(1024)(128)(2,1)S(1)}, bf16[2048]{0:T(1024)(128)(2,1)}, u32[]{:S(2)}) copy-start(bf16[2048]{0:T(1024)(128)(2,1)} %param.43) | copy-start | bytes 12292
  91.2 10.8 %copy-start.8 = (f32[2048,4]{0,1:T(4,128)S(1)}, f32[2048,4]{0,1:T(4,128)}, u32[]{:S(2)}) copy-start(f32[2048,4]{0,1:T(4,128)} %param.44) | copy-start | bytes 98308
  91.2 10.9 %copy-start.6 = (f32[2048,6]{0,1:T(8,128)S(1)}, f32[2048,6]{0,1:T(8,128)}, u32[]{:S(2)}) copy-start(f32[2048,6]{0,1:T(8,128)} %param.46) | copy-start | bytes 147460
  231.4 4.9 %copy-start.3 = (bf16[2048,16]{0,1:T(8,128)(2,1)S(1)}, bf16[2048,16]{0,1:T(8,128)(2,1)}, u32[]{:S(2)}) copy-start(bf16[2048,16]{0,1:T(8,128)(2,1)} %param.40) | copy-start | bytes 196612
  236.3 5.7 %copy-start.7 = (bf16[2048,16]{0,1:T(8,128)(2,1)S(1)}, bf16[2048,16]{0,1:T(8,128)(2,1)}, u32[]{:S(2)}) copy-start(bf16[2048,16]{0,1:T(8,128)(2,1)} %param.41) | copy-start | bytes 196612
  247.6 3.1 copy-start.15
  248.7 2.1 copy-start.14
  284.6 67.8 %all-to-all-start.2 = ((bf16[16,8,8,2048]{3,2,1,0:T(8,128)(2,1)}), bf16[16,8,8,2048]{3,2,1,0:T(8,128)(2,1)}, u32[]{:S(2)}, u32[]{:S(2)}) async-start(bf16[16,8,8,2048]{3,2,1,0:T(8,128)(2,1)} %copy.59), calls=%async_computation.2 | async-start | bytes 8388608 | tf_op jit(solution)/shard_map/all_to_all | solution.py:43
  356.1 13.6 %all-to-all-start.3 = ((bf16[8,8,2048]{2,1,0:T(8,128)(2,1)}), bf16[8,8,2048]{2,1,0:T(8,128)(2,1)S(1)}, u32[]{:S(2)}, u32[]{:S(2)}) async-start(bf16[8,8,2048]{2,1,0:T(8,128)(2,1)} %reduce_sum.140), calls=%async_computation.3 | async-start | bytes 524288 | tf_op jit(solution)/shard_map/all_to_all | solution.py:51
  360.0 10.4 %copy-start.1 = (bf16[1,2048,256]{2,1,0:T(8,128)(2,1)S(1)}, bf16[1,2048,256]{2,1,0:T(8,128)(2,1)}, u32[]{:S(2)}) copy-start(bf16[1,2048,256]{2,1,0:T(8,128)(2,1)} %param.48) | copy-start | bytes 3145732
Sparse Core Ops, SparseCore 0:
  29.2 61.9 all-gather.2
  100.0 118.7 all-gather.4
where the time goes:
time: 379 us; the launch traced here: 377 us
  waiting for transfers between devices  214 us (56%)
  blocking collectives  41.7 us (11%)
  other arithmetic  34.2 us (9%)
  local copies, waits for them, and re-layouts  33.5 us (9%)
  matrix products  30 us (8%)
  between operations  14.5 us (4%)
  starting transfers between devices  8.94 us (2%)
    all_gather x1, waiting for transfers between devices, shards(): gathered = lax.all_gather(normed, EP, axis=0, tiled=True)  115 us
    all_to_all x1, waiting for transfers between devices, sum_at_owner(): lax.all_to_all(split_up(shard, dim, devices), axis, 0, 0, tiled=True)  54.9 us
    all_gather x1, waiting for transfers between devices, gathered_by_axis(): nearer = lax.all_gather(shard, axes[-1], axis=dim, tiled=True)  41 us
    all_gather x2, blocking collectives, gathered_by_axis(): nearer = lax.all_gather(shard, axes[-1], axis=dim, tiled=True)  21.8 us
    all_to_all x1, blocking collectives, sum_at_owner(): lax.all_to_all(split_up(shard, dim, devices), axis, 0, 0, tiled=True)  15.6 us
    reduce_sum x2, other arithmetic, sum_at_owner(): return jnp.sum(pieces.astype(jnp.float32), axis=0)  12.5 us
    mul x1, other arithmetic, state_update(): (step_size[:, :, None] * x_heads)[:, :, :, None]  8.4 us
    mul x1, local copies, waits for them, and re-layouts, state_update(): (step_size[:, :, None] * x_heads)[:, :, :, None]  7.88 us
  transfers between devices with their start and end apart: 4, of which 4 were waited for; matrix products, arithmetic and copies ran while one was open for 10% of the time, Pallas kernels for 0%

commit v1 on v0

v1 whole, which is shorter than its diff:
```python
import functools

import jax
import jax.numpy as jnp
from jax import lax
from jax.experimental import pallas as pl
from jax.experimental.pallas import tpu as pltpu
from jax.sharding import Mesh
from jax.sharding import PartitionSpec as P

F32, BF16, I32 = jnp.float32, jnp.bfloat16, jnp.int32
EP = ("z", "y", "x")
EP_TP = ("z", "y", "x", "tp")
NZ, NY, NX = 8, 4, 4
EPSILON = 1e-06
MESH = pl.DeviceIdType.MESH
VMEM = pltpu.MemorySpace.VMEM
CHUNKS = 8


def dot(a, b):
    return lax.dot_general(a, b, (((1,), (0,)), ((), ())), preferred_element_type=F32)


def dot_t(a, b):
    return lax.dot_general(a, b, (((1,), (1,)), ((), ())), preferred_element_type=F32)


def silu(v):
    return v / (1.0 + jnp.exp(-v))


def iota(shape, dim):
    return lax.broadcasted_iota(I32, shape, dim)


def split(v):
    high = v.astype(BF16)
    return high, (v - high.astype(F32)).astype(BF16)


def spread(v, width):
    total = v.shape[1]
    heads = total // width
    per = 16 // heads
    mask = (iota((16, total), 1) // width) == (iota((16, total), 0) // per)
    rows = jnp.where(mask[None], jnp.broadcast_to(v[:, None, :], (16, 16, total)), 0.0).reshape(256, total)
    pick = ((iota((total, 128), 0) % width) == (iota((total, 128), 1) % width)).astype(BF16)
    high, low = split(rows)
    return dot(high, pick) + dot(low, pick)


def local_kernel(px, pz, bc, pdt, tx, wx, dtb, dlg, gg, ids, ew, gw, state, new_state, y_out, disp, c_hi, c_lo,
                 sbuf, route, xs_s, in_s, rd_s, de_s, rdo, isem, osem):
    def in_copy(j):
        return pltpu.make_async_copy(state.at[:, :, pl.ds(pl.multiple_of(j * 512, 512), 512)], sbuf.at[j], isem.at[j])

    def out_copy(j):
        return pltpu.make_async_copy(sbuf.at[j], new_state.at[:, :, pl.ds(pl.multiple_of(j * 512, 512), 512)], osem.at[j])

    for j in range(CHUNKS):
        in_copy(j).start()
    conv_x = px[...].astype(F32) * wx[3:4, :].astype(F32)
    for w in range(3):
        conv_x = conv_x + tx[w].astype(F32) * wx[w : w + 1, :].astype(F32)
    conv_x = silu(conv_x)
    pre = pdt[...].astype(F32) + dtb[...]
    step = jnp.maximum(pre, 0.0) + jnp.log1p(jnp.exp(-jnp.abs(pre)))
    decay = jnp.exp(-step * jnp.exp(dlg[...]))
    eye = (iota((16, 16), 0) == iota((16, 16), 1))[None]

    def column(v):
        wide = jnp.where(eye, jnp.broadcast_to(v[:, None, :], (16, 16, 16)), 0.0)
        return jnp.sum(wide, axis=-1, keepdims=True).reshape(256, 1)

    x_rows = spread(conv_x, 64) * column(step)
    high, low = split(x_rows)
    xs_s[...] = jnp.where(iota((256, 128), 1) < 64, high.astype(F32), low.astype(F32)).astype(BF16)
    in_s[...] = spread(bc[0], 64)
    rd_s[...] = spread(bc[1], 64)
    de_s[...] = jnp.broadcast_to(column(decay), (256, 128))
    rdo[...] = jnp.zeros_like(rdo)

    def chunk(j, carry):
        in_copy(j).wait()
        grid = ((iota((128, 512), 0) % 64) == (iota((128, 512), 1) // 64 + j * 8)).astype(BF16)
        fresh = dot(xs_s[...], grid)
        old = sbuf[j].reshape(256, 512)
        new = jnp.tile(de_s[...], (1, 4)) * old + fresh * jnp.tile(in_s[...], (1, 4))
        sbuf[j] = new.reshape(16, 16, 512)
        rdo[...] += dot_t((new * jnp.tile(rd_s[...], (1, 4))).astype(BF16), grid)
        return carry

    def chunk_out(j, carry):
        chunk(j, carry)
        out_copy(j).start()
        return carry

    lax.fori_loop(0, CHUNKS, chunk_out, 0)

    wide = jnp.tile(rdo[...], (1, 8))
    keep = (iota((16, 1024), 1) // 64) == iota((16, 1024), 0)
    read = jnp.sum(jnp.where(keep[None], wide.reshape(16, 16, 1024), 0.0), axis=1)
    gated = read * silu(pz[...].astype(F32))
    for g in range(4):
        part = gated[:, g * 256 : (g + 1) * 256]
        scale = lax.rsqrt(jnp.mean(part * part, axis=-1, keepdims=True) + EPSILON)
        y_out[:, g * 256 : (g + 1) * 256] = (part * scale * gg[:, g * 256 : (g + 1) * 256]).astype(BF16)

    z, q = lax.axis_index("z"), lax.axis_index("y") * NX + lax.axis_index("x")
    route[...] = jnp.zeros_like(route)
    route[0:6, :] = ids[...].astype(F32)
    route[8:14, :] = ew[...]
    route[16:20, :] = gw[...]
    row, tok = iota((2048, 128), 0), iota((2048, 128), 1)
    take = (row == (tok // 16) * 256 + q * 16 + tok % 16).astype(BF16)
    high, rest = split(route[...])
    mine = dot(high, take) + dot(rest, take)
    own = iota((16, 128), 0) + z * 16
    hit = jnp.zeros((16, 128), F32)
    weight = jnp.zeros((16, 128), F32)
    for k in range(6):
        same = mine[k : k + 1, :].astype(I32) == own
        hit = hit + same.astype(F32)
        weight = weight + jnp.where(same, mine[8 + k : 9 + k, :], 0.0)
    coarse = jnp.sum(jnp.where(iota((8, 128), 0) == z // 2, mine[16:24, :], 0.0), axis=0, keepdims=True)
    weight = weight * coarse
    a, b = iota((128, 128), 0), iota((128, 128), 1)
    before = ((a // 16 == b // 16) & (a < b)).astype(BF16)
    rank = dot(hit.astype(BF16), before)
    slot, tok3 = iota((16, 16, 128), 1), iota((16, 16, 128), 2)
    chosen = (
        (hit[:, None, :] > 0.5)
        & (rank[:, None, :] == (slot % 2).astype(F32))
        & (slot // 2 == tok3 // 16)
    )
    disp[...] = jnp.where(chosen, 1.0, 0.0).reshape(256, 128).astype(BF16)
    comb = jnp.where(chosen, jnp.broadcast_to(weight[:, None, :], (16, 16, 128)), 0.0).reshape(256, 128)
    comb = jnp.concatenate([comb[:128].T, comb[128:].T], axis=1)
    high, low = split(comb)
    c_hi[...] = high
    c_lo[...] = low
    for j in range(CHUNKS):
        out_copy(j).wait()


class Copies:
    def __init__(self, sems):
        self.sems, self.started = sems, []

    def __call__(self, src, dst, recv, **where):
        copy = pltpu.make_async_remote_copy(
            src_ref=src, dst_ref=dst, send_sem=self.sems.at[len(self.started)], recv_sem=recv,
            device_id=where, device_id_type=MESH,
        )
        copy.start()
        self.started.append(copy)

    def arrived(self, ref, recv, **where):
        pltpu.make_async_remote_copy(
            src_ref=ref, dst_ref=ref, send_sem=self.sems.at[0], recv_sem=recv, device_id=where, device_id_type=MESH,
        ).wait_recv()

    def drain(self):
        for copy in self.started:
            copy.wait_send()


def plane_gather(copies, buf, lane, width, g, rsem, coords):
    fa, sa = ("x", "y") if g == 0 else ("y", "x")
    f, s = coords[fa], coords[sa]

    def place(df, ds):
        fv, sv = lax.rem(f + df + 4, 4), lax.rem(s + ds + 4, 4)
        return sv * 4 + fv if g == 0 else fv * 4 + sv

    def piece(qi, part):
        start, size = (lane, width) if part == 0 else (lane + (part - 1) * (width // 2), width // 2)
        lead = (qi,) + (slice(None),) * (len(buf.shape) - 2)
        return buf.at[lead + (pl.ds(start, size),)]

    def send(df, ds, part, axis, move):
        qi = place(df, ds)
        ref = piece(qi, part)
        copies(ref, ref, rsem.at[g, qi, 1 if part == 2 else 0], **{axis: lax.rem(coords[axis] + move + 4, 4)})

    def wait(df, ds, part):
        qi = place(df, ds)
        copies.arrived(piece(qi, part), rsem.at[g, qi, 1 if part == 2 else 0], **{fa: lax.rem(f + 1, 4)})

    for move in (1, -1):
        send(0, 0, 0, fa, move)
    for move in (1, -1):
        send(0, 0, 0, sa, move)
    yield
    for df, part in ((-1, 1), (1, 2)):
        wait(df, 0, 0)
        send(df, 0, part, fa, -df)
        for move in (1, -1):
            send(df, 0, 0, sa, move)
    yield
    wait(2, 0, 1)
    wait(2, 0, 2)
    for move in (1, -1):
        send(2, 0, 0, sa, move)
    yield
    for df in (0, -1, 1, 2):
        for ds, part in ((-1, 1), (1, 2)):
            wait(df, ds, 0)
            send(df, ds, part, sa, -ds)
    yield
    for df in (0, -1, 1, 2):
        wait(df, 2, 1)
        wait(df, 2, 2)
    yield


Z_ORDER = (4, 3, 5, 2, 6, 1, 7)
PLANE_ORDER = ((2, 2), (1, 2), (3, 2), (2, 1), (2, 3), (2, 0), (0, 2), (1, 1), (1, 3), (3, 1), (3, 3), (1, 0), (3, 0), (0, 1), (0, 3))


def mesh_kernel(y_ref, r_ref, ot_ref, gt_ref, ut_ref, dn_ref, gain, bgate, disp, c_hi, c_lo, eg_hbm, eu_hbm, ed_hbm, out_ref,
                wbuf, obuf, ybuf, rbuf, mown, msend, mrecv, nbuf, rn, normed, dsend, drecv, xsend, xfull, esend, erecv,
                csend, cbuf, tot, zsend, zrecv, fin, frecv, eg, eu, ed,
                ssem, wsem, gsem, zsem, asem, tsem, nsem, fsem, lsem):
    z, y, x, t = (lax.axis_index(a) for a in EP_TP)
    coords = {"x": x, "y": y}
    q = y * 4 + x
    other = 1 - t
    planes = [(lax.rem(y + dy, 4), lax.rem(x + dx, 4)) for dy, dx in PLANE_ORDER]
    zs = [lax.rem(z + d, 8) for d in Z_ORDER]

    loads = [pltpu.make_async_copy(src.at[0], dst, lsem.at[i]) for i, (src, dst) in enumerate(((eg_hbm, eg), (eu_hbm, eu), (ed_hbm, ed)))]
    for load in loads:
        load.start()

    barrier = pltpu.get_barrier_semaphore()
    for zz in zs:
        pl.semaphore_signal(barrier, inc=1, device_id={"z": zz}, device_id_type=MESH)
    for yy, xx in planes:
        pl.semaphore_signal(barrier, inc=1, device_id={"y": yy, "x": xx}, device_id_type=MESH)
    pl.semaphore_signal(barrier, inc=1, device_id={"tp": other}, device_id_type=MESH)
    obuf[q] = ot_ref[...]
    wbuf[q, 0] = gt_ref[...]
    wbuf[q, 1] = ut_ref[...]
    wbuf[q, 2] = dn_ref[...]
    ybuf[z] = y_ref[...]
    pl.semaphore_wait(barrier, len(zs) + len(planes) + 1)

    copies = Copies(ssem)
    for zz in zs:
        copies(y_ref, ybuf.at[z], zsem.at[0, z], z=zz)
    for zz in zs:
        copies(r_ref.at[:, pl.ds(pl.multiple_of(zz * 256 + t * 128, 128), 128)], rbuf.at[z], zsem.at[1, z], z=zz)
    og = [plane_gather(copies, obuf, g * 512, 512, g, gsem, coords) for g in range(2)]
    wg = [plane_gather(copies, wbuf, g * 1024, 1024, g, wsem, coords) for g in range(2)]

    def advance(gens):
        for gen in gens:
            next(gen)

    advance(og)
    advance(wg)
    rbuf[z] = r_ref[:, pl.ds(pl.multiple_of(z * 256 + t * 128, 128), 128)]
    advance(og)
    advance(og)
    advance(wg)
    advance(og)
    advance(og)
    for zz in zs:
        copies.arrived(ybuf.at[zz], zsem.at[0, zz], z=zz)

    rows = ybuf[...].reshape(128, 1024)
    mown[...] = dot_t(rows, obuf[pl.ds(t * 8, 8)].reshape(128, 1024))
    msend[...] = dot_t(rows, obuf[pl.ds(other * 8, 8)].reshape(128, 1024)).astype(BF16)
    copies(msend, mrecv, tsem.at[0], tp=other)
    advance(wg)
    for zz in zs:
        copies.arrived(rbuf.at[zz], zsem.at[1, zz], z=zz)
    copies.arrived(mrecv, tsem.at[0], tp=other)
    mixed = mown[...] + mrecv[...].astype(F32)
    nbuf[z, t] = (rbuf[...].reshape(128, 128).astype(F32) + mixed).astype(BF16)
    for zz in zs:
        copies(nbuf.at[z, t], nbuf.at[z, t], zsem.at[2, z], z=zz)
    copies(nbuf.at[z, t], nbuf.at[z, t], nsem.at[z], tp=other)
    advance(wg)
    for zz in zs[::-1]:
        copies.arrived(nbuf.at[zz, t], zsem.at[2, zz], z=zz)
        copies(nbuf.at[zz, t], nbuf.at[zz, t], nsem.at[zz], tp=other)
    for zz in zs[::-1] + [z]:
        copies.arrived(nbuf.at[zz, other], nsem.at[zz], tp=other)

    for j in range(16):
        rn[:, j * 128 : (j + 1) * 128] = nbuf[j // 2, j % 2]
    wide = rn[...].astype(F32)
    scale = lax.rsqrt(jnp.mean(wide * wide, axis=-1, keepdims=True) + EPSILON)
    normed[...] = (wide * scale * gain[...]).astype(BF16)
    half = pl.ds(pl.multiple_of(t * 1024, 1024), 1024)
    far = pl.ds(pl.multiple_of(other * 1024, 1024), 1024)

    xsend[...] = dot(disp[...], normed[:, half]).astype(BF16).reshape(16, 16, 1024)
    for yy, xx in planes:
        copies(xsend.at[yy * 4 + xx], xfull.at[t, q], asem.at[0, q], y=yy, x=xx)
    xfull[t, q] = xsend[q]
    copies(xsend.at[q], xfull.at[t, q], fsem.at[q], tp=other)

    advance(wg)
    tokens = normed[...]
    score = jnp.sum(tokens.astype(F32) * bgate[...].astype(F32), axis=-1, keepdims=True)
    gate = dot_t(tokens, wbuf[:, 0].reshape(256, 2048))
    lin = dot_t(tokens, wbuf[:, 1].reshape(256, 2048))
    hidden = (silu(gate) * lin / (1.0 + jnp.exp(-score))).astype(BF16)
    dsend[...] = dot(hidden, wbuf[:, 2, :, far].reshape(256, 1024)).astype(BF16)
    copies(dsend, drecv, tsem.at[1], tp=other)
    tot[...] = dot(hidden, wbuf[:, 2, :, half].reshape(256, 1024)).reshape(8, 16, 1024)

    for yy, xx in planes[::-1]:
        qq = yy * 4 + xx
        copies.arrived(xfull.at[t, qq], asem.at[0, qq], y=yy, x=xx)
        copies(xfull.at[t, qq], xfull.at[t, qq], fsem.at[qq], tp=other)
    for yy, xx in planes[::-1] + [(y, x)]:
        qq = yy * 4 + xx
        copies.arrived(xfull.at[other, qq], fsem.at[qq], tp=other)
    for load in loads:
        load.wait()
    left, right = xfull[0].reshape(256, 1024), xfull[1].reshape(256, 1024)
    gate = dot(left, eg[0:1024, :]) + dot(right, eg[1024:2048, :])
    lin = dot(left, eu[0:1024, :]) + dot(right, eu[1024:2048, :])
    hidden = (silu(gate) * lin).astype(BF16)
    esend[...] = dot(hidden, ed[:, far]).astype(BF16)
    copies(esend, erecv, tsem.at[2], tp=other)
    mine = dot(hidden, ed[:, half])
    copies.arrived(erecv, tsem.at[2], tp=other)
    csend[...] = (mine + erecv[...].astype(F32)).astype(BF16).reshape(16, 16, 1024)
    for yy, xx in planes:
        copies(csend.at[yy * 4 + xx], cbuf.at[q], asem.at[1, q], y=yy, x=xx)
    cbuf[q] = csend[q]
    copies.arrived(drecv, tsem.at[1], tp=other)
    tot[...] = tot[...] + drecv[...].astype(F32).reshape(8, 16, 1024)
    for yy, xx in planes[::-1]:
        qq = yy * 4 + xx
        copies.arrived(cbuf.at[qq], asem.at[1, qq], y=yy, x=xx)
    back = cbuf[...].reshape(256, 1024)
    total = tot[...].reshape(128, 1024) + dot(c_hi[...], back) + dot(c_lo[...], back)
    tot[...] = total.reshape(8, 16, 1024)
    zsend[...] = total.astype(BF16).reshape(8, 16, 1024)
    for zz in zs:
        copies(zsend.at[zz], zrecv.at[z], zsem.at[3, z], z=zz)
    final = tot[z] + rn[pl.ds(pl.multiple_of(z * 16, 16), 16), half].astype(F32)
    for zz in zs[::-1]:
        copies.arrived(zrecv.at[zz], zsem.at[3, zz], z=zz)
        final = final + zrecv[zz].astype(F32)
    fin[...] = final
    copies(fin.at[pl.ds(pl.multiple_of(other * 8, 8), 8)], frecv, tsem.at[3], tp=other)
    out_ref[:, half] = fin[pl.ds(pl.multiple_of(t * 8, 8), 8), :].astype(BF16)
    copies.arrived(frecv, tsem.at[3], tp=other)
    out_ref[:, far] = frecv[...].astype(BF16)
    copies.drain()


def shards(resid, proj_x, proj_z, proj_bc, proj_dt, tail_x, tail_bc, taps_x, taps_bc, ssm_state, dt_bias, decay_log,
           group_gain, out_proj, ffn_gain, dense_gate, dense_up, dense_down, branch_gate, group_weights, expert_ids,
           expert_weights, exp_gate, exp_up, exp_down):
    window = jnp.concatenate([tail_bc, proj_bc[:, None]], axis=1).astype(F32)
    bc = jax.nn.silu(jnp.sum(window * taps_bc.astype(F32)[None], axis=1)).transpose(1, 0, 2)
    vm = pl.BlockSpec(memory_space=VMEM)
    hbm = pl.BlockSpec(memory_space=pl.ANY)
    new_state, y_out, disp, c_hi, c_lo = pl.pallas_call(
        local_kernel,
        out_shape=(
            jax.ShapeDtypeStruct((16, 16, 4096), F32),
            jax.ShapeDtypeStruct((16, 1024), BF16),
            jax.ShapeDtypeStruct((256, 128), BF16),
            jax.ShapeDtypeStruct((128, 256), BF16),
            jax.ShapeDtypeStruct((128, 256), BF16),
        ),
        in_specs=[vm] * 12 + [hbm],
        out_specs=(hbm, vm, vm, vm, vm),
        scratch_shapes=[
            pltpu.VMEM((CHUNKS, 16, 16, 512), F32),
            pltpu.VMEM((32, 2048), F32),
            pltpu.VMEM((256, 128), BF16),
            pltpu.VMEM((256, 128), F32),
            pltpu.VMEM((256, 128), F32),
            pltpu.VMEM((256, 128), F32),
            pltpu.VMEM((256, 128), F32),
            pltpu.SemaphoreType.DMA((CHUNKS,)),
            pltpu.SemaphoreType.DMA((CHUNKS,)),
        ],
        compiler_params=pltpu.CompilerParams(vmem_limit_bytes=32 << 20),
        name="state",
    )(proj_x, proj_z, bc, proj_dt, tail_x.transpose(1, 0, 2), taps_x, dt_bias.reshape(1, 16), decay_log.reshape(1, 16),
      group_gain.reshape(1, 1024), expert_ids.T, expert_weights.T, group_weights.T, ssm_state)
    out = pl.pallas_call(
        mesh_kernel,
        out_shape=jax.ShapeDtypeStruct((8, 2048), BF16),
        in_specs=[vm] * 11 + [hbm] * 3,
        out_specs=vm,
        scratch_shapes=[
            pltpu.VMEM((16, 3, 16, 2048), BF16),
            pltpu.VMEM((16, 16, 1024), BF16),
            pltpu.VMEM((8, 16, 1024), BF16),
            pltpu.VMEM((8, 16, 128), BF16),
            pltpu.VMEM((128, 128), F32),
            pltpu.VMEM((128, 128), BF16),
            pltpu.VMEM((128, 128), BF16),
            pltpu.VMEM((8, 2, 128, 128), BF16),
            pltpu.VMEM((128, 2048), BF16),
            pltpu.VMEM((128, 2048), BF16),
            pltpu.VMEM((128, 1024), BF16),
            pltpu.VMEM((128, 1024), BF16),
            pltpu.VMEM((16, 16, 1024), BF16),
            pltpu.VMEM((2, 16, 16, 1024), BF16),
            pltpu.VMEM((256, 1024), BF16),
            pltpu.VMEM((256, 1024), BF16),
            pltpu.VMEM((16, 16, 1024), BF16),
            pltpu.VMEM((16, 16, 1024), BF16),
            pltpu.VMEM((8, 16, 1024), F32),
            pltpu.VMEM((8, 16, 1024), BF16),
            pltpu.VMEM((8, 16, 1024), BF16),
            pltpu.VMEM((16, 1024), F32),
            pltpu.VMEM((8, 1024), F32),
            pltpu.VMEM((2048, 256), BF16),
            pltpu.VMEM((2048, 256), BF16),
            pltpu.VMEM((256, 2048), BF16),
            pltpu.SemaphoreType.DMA((192,)),
            pltpu.SemaphoreType.DMA((2, 16, 2)),
            pltpu.SemaphoreType.DMA((2, 16, 2)),
            pltpu.SemaphoreType.DMA((4, 8)),
            pltpu.SemaphoreType.DMA((2, 16)),
            pltpu.SemaphoreType.DMA((4,)),
            pltpu.SemaphoreType.DMA((8,)),
            pltpu.SemaphoreType.DMA((16,)),
            pltpu.SemaphoreType.DMA((3,)),
        ],
        compiler_params=pltpu.CompilerParams(collective_id=0, has_side_effects=True, vmem_limit_bytes=48 << 20),
        name="mesh",
    )(y_out, resid, out_proj.T, dense_gate.T, dense_up.T, dense_down, ffn_gain.reshape(1, 2048),
      branch_gate.reshape(1, 2048), disp, c_hi, c_lo, exp_gate, exp_up, exp_down)
    return (out, new_state)


def solution(mesh):
    finer = Mesh(mesh.devices.reshape(NZ, NY, NX, mesh.shape["tp"]), EP_TP)
    in_specs = (
        P(EP, None), P(EP, "tp"), P(EP, "tp"), P(EP, None, "tp"), P(EP, "tp"), P(EP, None, "tp"), P(EP, None, None, "tp"),
        P(None, "tp"), P(None, None, "tp"), P(EP, "tp", None), P("tp"), P("tp"), P("tp"), P("tp", EP), P(),
        P(None, EP_TP), P(None, EP_TP), P(EP_TP, None), P(), P(), P(), P(), P(EP, None, "tp"), P(EP, None, "tp"),
        P(EP, "tp", None),
    )
    out_specs = (P(EP_TP, None), P(EP, "tp", None))
    return jax.shard_map(shards, mesh=finer, in_specs=in_specs, out_specs=out_specs, check_vma=False)
```

time: 379 us -> 89.9 us (0.24)
  waiting for transfers between devices: 214 us -> 0 us
  Pallas kernels: 0 us -> 74.9 us
  blocking collectives: 41.7 us -> 0 us
  other arithmetic: 34.2 us -> 1.7 us
  matrix products: 30 us -> 0 us
  local copies, waits for them, and re-layouts: 33.5 us -> 11.8 us
  between operations: 14.5 us -> 0.79 us
  starting transfers between devices: 8.94 us -> 0 us
    all_gather x2 -> x0, waiting for transfers between devices: 156 us -> none  [the longest x1 115 us: shards(): gathered = lax.all_gather(normed, EP, axis=0, tiled=True)]
    pallas_call x0 -> x2, Pallas kernels: none -> 74.9 us  [the longest x1 70.3 us: shards(): pl.pallas_call(mesh_kernel, out_shape=jax.ShapeDtypeStruct((8, 2048), BF1...]
    all_to_all x2 -> x0, waiting for transfers between devices: 58 us -> none  [the longest x1 54.9 us: sum_at_owner(): lax.all_to_all(split_up(shard, dim, devices), axis, 0, 0, tiled=True)]
    dot_general x7 -> x0, matrix products: 30 us -> none  [the longest x1 5.68 us: shards(): jnp.dot(gathered, dense_gate, preferred_element_type=jnp.float32)]
    all_gather x2 -> x0, blocking collectives: 21.8 us -> none  [gathered_by_axis(): nearer = lax.all_gather(shard, axes[-1], axis=dim, tiled=True)]
    all_to_all x2 -> x0, blocking collectives: 19.9 us -> none  [the longest x1 15.6 us: sum_at_owner(): lax.all_to_all(split_up(shard, dim, devices), axis, 0, 0, tiled=True)]
    reduce_sum x11 -> x1, other arithmetic: 15 us -> 0.93 us  [shards(): jnp.sum(window * taps_bc.astype(F32)[None], axis=1)]
    unnamed x34 -> x43, local copies, waits for them, and re-layouts: 0.1 us -> 11.1 us
  transfers between devices with their start and end apart: 4 -> 0, of which waited for: 4 -> 0; matrix products, arithmetic and copies ran while one was open for 10% -> 0% of each run, Pallas kernels for 0% -> 0%
where the time goes in v1:
time: 89.9 us; the launch traced here: 89.2 us
  Pallas kernels  74.9 us (83%)
  local copies, waits for them, and re-layouts  11.8 us (13%)
  other arithmetic  1.7 us (2%)
    pallas_call x1, Pallas kernels, shards(): pl.pallas_call(mesh_kernel, out_shape=jax.ShapeDtypeStruct((8, 2048), BF1...  70.3 us
    unnamed x43, local copies, waits for them, and re-layouts  11.1 us
    pallas_call x1, Pallas kernels, shards(): pl.pallas_call(local_kernel, out_shape=(jax.ShapeDtypeStruct((16, 16, 409...  4.65 us

profile of v1, /device:TPU:1, one launch (start us, length us, event | category | flops | bytes accessed | tf_op | source)
XLA Modules:
  0.0 89.2 jit_solution(2696348918246151935)
XLA Ops:
  0.6 0.0 copy-start.9
  0.6 0.0 copy-start.8
  0.7 0.0 copy-start.16
  0.7 0.0 copy-start.7
  0.7 0.8 convert_element_type.7
  1.4 0.7 reshape.24.bgate
  2.1 0.9 %multiply_reduce_fusion = f32[16,2,256]{2,1,0:T(2,128)S(1)} fusion(bf16[16,1,2,256]{3,2,1,0:T(2,128)(2,1)} %bitcast.34, bf16[16,3,2,256]{3,2,1,0:T(2,128)(2,1)} %param.31, f32[4,2,256]{2,1,0:T(2,128)S(1)} %convert_element_type.7), kind=kLoop, calls=%fused_computation | loop fusion | flops 122880 | bytes 106496 | tf_op jit(solution)/shard_map/reduce_sum | solution.py:365
  3.1 0.0 copy-start
  3.1 2.2 %copy-done = f32[16,16,4096]{2,1,0:T(8,128)S(1)} copy-done((f32[16,16,4096]{2,1,0:T(8,128)S(1)}, f32[16,16,4096]{2,1,0:T(8,128)}, u32[]{:S(2)}) %copy-start) | copy-done | bytes 4194328
  5.3 0.0 copy-start.4
  5.3 0.9 copy-done.4
  6.2 0.0 copy-start.5
  6.2 0.8 copy-done.5
  7.0 0.0 copy-start.6
  7.0 0.8 copy-done.6
  7.8 0.0 copy-start.11
  7.8 0.8 copy-done.11
  8.6 0.0 copy-start.12
  8.6 0.8 copy-done.12
  9.4 0.0 copy-start.13
  9.4 0.8 copy-done.13
  10.1 0.0 copy-start.15
  10.1 0.7 copy-done.15
  10.8 0.0 copy-start.17
  10.8 0.7 copy-done.17
  11.5 0.0 copy-start.18
  11.5 0.7 copy-done.18
  12.2 0.0 copy-start.19
  12.2 0.7 copy-done.19
  12.8 0.0 copy-start.20
  12.8 0.7 copy-done.20
  13.5 0.0 copy-start.1
  13.5 0.0 copy-start.2
  13.5 0.0 copy-start.3
  13.5 0.0 copy-start.10
  13.5 0.0 copy-start.14
  13.5 4.6 %state.2 = (f32[16,16,4096]{2,1,0:T(8,128)}, bf16[16,1024]{1,0:T(8,128)(2,1)S(1)}, bf16[256,128]{1,0:T(8,128)(2,1)S(1)}, bf16[128,256]{1,0:T(8,128)(2,1)S(1)}, bf16[128,256]{1,0:T(8,128)(2,1)S(1)}) custom-call(bf16[16,1024]{1,0:T(8,128)(2,1)S(1)} %copy-done.11, bf16[16,1024]{1,0:T(8,128)(2,1)S(1)} %copy-done.12, f32[2,16,256]{2,1,0:T(8,128)S(1)} %bitcast_multiply_fusion.bc, ...), custom_call_target="tpu_custom_call" | custom-call | tf_op jit(solution)/shard_map/state/pallas_call | solution.py:368
  18.2 0.0 copy-done.9
  18.2 0.0 copy-done.8
  18.2 0.0 copy-done.16
  18.2 0.0 copy-done.7
  18.2 0.0 copy-done.1
  18.2 0.0 copy-done.2
  18.2 0.0 copy-done.3
  18.2 0.0 copy-done.10
  18.3 0.0 copy-done.14
  18.3 70.3 %mesh.1 = bf16[8,2048]{1,0:T(8,128)(2,1)S(1)} custom-call(bf16[16,1024]{1,0:T(8,128)(2,1)S(1)} %get-tuple-element.7.y_ref, bf16[16,2048]{1,0:T(8,128)(2,1)S(1)} %copy-done.7, bf16[16,1024]{1,0:T(8,128)(2,1)S(1)} %bitcast.29, bf16[16,2048]{1,0:T(8,128)(2,1)S(1)} %bitcast.26, bf16[16,2048]{1,0:T(8,128)(2,1)S(1)} %bitcast.27, bf16[16,2048]{1,0:T(8,128)(2,1)S(1)} %copy-done.10, ...), custom_call_target="tpu_custom_call" | custom-call | tf_op jit(solution)/shard_map/mesh/pallas_call | solution.py:394
  88.5 0.6 copy.30
  (1 shorter events, 0.0 us)
Async XLA Ops:
  0.6 17.5 %copy-start.9 = (bf16[2048,16]{0,1:T(8,128)(2,1)S(1)}, bf16[2048,16]{0,1:T(8,128)(2,1)}, u32[]{:S(2)}) copy-start(bf16[2048,16]{0,1:T(8,128)(2,1)} %param.41) | copy-start | bytes 196612
  0.6 17.5 %copy-start.8 = (bf16[2048,16]{0,1:T(8,128)(2,1)S(1)}, bf16[2048,16]{0,1:T(8,128)(2,1)}, u32[]{:S(2)}) copy-start(bf16[2048,16]{0,1:T(8,128)(2,1)} %param.40) | copy-start | bytes 196612
  0.7 17.5 %copy-start.16 = (f32[2048]{0:T(1024)S(1)}, f32[2048]{0:T(1024)}, u32[]{:S(2)}) copy-start(f32[2048]{0:T(1024)} %param.39) | copy-start | bytes 24580
  0.7 17.5 %copy-start.7 = (bf16[16,2048]{1,0:T(8,128)(2,1)S(1)}, bf16[16,2048]{1,0:T(8,128)(2,1)}, u32[]{:S(2)}) copy-start(bf16[16,2048]{1,0:T(8,128)(2,1)} %r_ref.1) | copy-start | bytes 196612
  3.1 2.2 %copy-start = (f32[16,16,4096]{2,1,0:T(8,128)S(1)}, f32[16,16,4096]{2,1,0:T(8,128)}, u32[]{:S(2)}) copy-start(f32[16,16,4096]{2,1,0:T(8,128)} %state.3) | copy-start | bytes 12582916
  5.3 0.9 %copy-start.4 = (bf16[16,3,1024]{2,0,1:T(8,128)(2,1)S(1)}, bf16[16,3,1024]{2,0,1:T(8,128)(2,1)}, u32[]{:S(2)}) copy-start(bf16[16,3,1024]{2,0,1:T(8,128)(2,1)} %param.30) | copy-start | bytes 294916
  6.2 0.8 copy-start.5
  7.0 0.8 copy-start.6
  7.8 0.8 copy-start.11
  8.6 0.8 copy-start.12
  9.4 0.8 copy-start.13
  10.1 0.7 copy-start.15
  10.8 0.7 copy-start.17
  11.5 0.7 copy-start.18
  12.2 0.7 copy-start.19
  12.8 0.7 copy-start.20
  13.5 4.7 %copy-start.1 = (bf16[1,2048,256]{2,1,0:T(8,128)(2,1)S(1)}, bf16[1,2048,256]{2,1,0:T(8,128)(2,1)}, u32[]{:S(2)}) copy-start(bf16[1,2048,256]{2,1,0:T(8,128)(2,1)} %eg_hbm.1) | copy-start | bytes 3145732
  13.5 4.7 %copy-start.2 = (bf16[1,2048,256]{2,1,0:T(8,128)(2,1)S(1)}, bf16[1,2048,256]{2,1,0:T(8,128)(2,1)}, u32[]{:S(2)}) copy-start(bf16[1,2048,256]{2,1,0:T(8,128)(2,1)} %eu_hbm.1) | copy-start | bytes 3145732
  13.5 4.7 %copy-start.3 = (bf16[1,256,2048]{2,1,0:T(8,128)(2,1)S(1)}, bf16[1,256,2048]{2,1,0:T(8,128)(2,1)}, u32[]{:S(2)}) copy-start(bf16[1,256,2048]{2,1,0:T(8,128)(2,1)} %ed_hbm.1) | copy-start | bytes 3145732
  13.5 4.7 %copy-start.10 = (bf16[16,2048]{1,0:T(8,128)(2,1)S(1)}, bf16[16,2048]{1,0:T(8,128)(2,1)}, u32[]{:S(2)}) copy-start(bf16[16,2048]{1,0:T(8,128)(2,1)} %dn_ref.1) | copy-start | bytes 196612
  13.5 4.8 %copy-start.14 = (bf16[1024,16]{0,1:T(8,128)(2,1)S(1)}, bf16[1024,16]{0,1:T(8,128)(2,1)}, u32[]{:S(2)}) copy-start(bf16[1024,16]{0,1:T(8,128)(2,1)} %param.38) | copy-start | bytes 98308

commit v2 on v1

v2 whole, which is shorter than its diff:
```python
import functools

import jax
import jax.numpy as jnp
from jax import lax
from jax.experimental import pallas as pl
from jax.experimental.pallas import tpu as pltpu
from jax.sharding import Mesh
from jax.sharding import PartitionSpec as P

F32, BF16, I32 = jnp.float32, jnp.bfloat16, jnp.int32
EP = ("z", "y", "x")
EP_TP = ("z", "y", "x", "tp")
NZ, NY, NX = 8, 4, 4
EPSILON = 1e-06
MESH = pl.DeviceIdType.MESH
VMEM = pltpu.MemorySpace.VMEM
CHUNKS = 4
WIDE = 4096 // CHUNKS
EARLY = 11
SMALL = 14


def dot(a, b):
    return lax.dot_general(a, b, (((1,), (0,)), ((), ())), preferred_element_type=F32)


def dot_t(a, b):
    return lax.dot_general(a, b, (((1,), (1,)), ((), ())), preferred_element_type=F32)


def silu(v):
    return v / (1.0 + jnp.exp(-v))


def iota(shape, dim):
    return lax.broadcasted_iota(I32, shape, dim)


def split(v):
    high = v.astype(BF16)
    return high, (v - high.astype(F32)).astype(BF16)


def spread(v):
    total = v.shape[1]
    per = 8 // (total // 64)
    mask = (iota((8, total), 1) // 64) == (iota((8, total), 0) // per)
    rows = jnp.where(mask[None], jnp.broadcast_to(v[:, None, :], (16, 8, total)), 0.0).reshape(128, total)
    pick = ((iota((total, 128), 0) % 64) == (iota((total, 128), 1) % 64)).astype(BF16)
    high, low = split(rows)
    return dot(high, pick) + dot(low, pick)


def column(v, half):
    mine = (iota((8, 16), 1) == iota((8, 16), 0) + half * 8)[None]
    wide = jnp.where(mine, jnp.broadcast_to(v[:, None, :], (16, 8, 16)), 0.0)
    return jnp.sum(wide, axis=-1, keepdims=True).reshape(128, 1)


class Copies:
    def __init__(self, sems):
        self.sems, self.started = sems, []

    def __call__(self, src, dst, recv, **where):
        copy = pltpu.make_async_remote_copy(
            src_ref=src, dst_ref=dst, send_sem=self.sems.at[len(self.started)], recv_sem=recv,
            device_id=where, device_id_type=MESH,
        )
        copy.start()
        self.started.append(copy)

    def arrived(self, ref, recv, **where):
        pltpu.make_async_remote_copy(
            src_ref=ref, dst_ref=ref, send_sem=self.sems.at[0], recv_sem=recv, device_id=where, device_id_type=MESH,
        ).wait_recv()

    def drain(self):
        for copy in self.started:
            copy.wait_send()


def plane_gather(copies, buf, lane, width, g, rsem, coords):
    fa, sa = ("x", "y") if g == 0 else ("y", "x")
    f, s = coords[fa], coords[sa]

    def place(df, ds):
        fv, sv = lax.rem(f + df + 4, 4), lax.rem(s + ds + 4, 4)
        return sv * 4 + fv if g == 0 else fv * 4 + sv

    def piece(qi, part):
        start, size = (lane, width) if part == 0 else (lane + (part - 1) * (width // 2), width // 2)
        lead = (qi,) + (slice(None),) * (len(buf.shape) - 2)
        return buf.at[lead + (pl.ds(start, size),)]

    def send(df, ds, part, axis, move):
        qi = place(df, ds)
        ref = piece(qi, part)
        copies(ref, ref, rsem.at[g, qi, 1 if part == 2 else 0], **{axis: lax.rem(coords[axis] + move + 4, 4)})

    def wait(df, ds, part):
        qi = place(df, ds)
        copies.arrived(piece(qi, part), rsem.at[g, qi, 1 if part == 2 else 0], **{fa: lax.rem(f + 1, 4)})

    turns = ((-1, 1), (1, 2))
    for axis in (fa, sa):
        for move in (1, -1):
            send(0, 0, 0, axis, move)
    yield
    for df, part in turns:
        wait(df, 0, 0)
        send(df, 0, part, fa, -df)
    for ds, part in turns:
        wait(0, ds, 0)
        send(0, ds, part, sa, -ds)
    yield
    for df in (-1, 1):
        for move in (1, -1):
            send(df, 0, 0, sa, move)
    yield
    wait(2, 0, 1)
    wait(2, 0, 2)
    for move in (1, -1):
        send(2, 0, 0, sa, move)
    for df in (-1, 1):
        for ds, part in turns:
            wait(df, ds, 0)
            send(df, ds, part, sa, -ds)
    yield
    for ds, part in turns:
        wait(2, ds, 0)
        send(2, ds, part, sa, -ds)
    yield
    for df in (0, -1, 1, 2):
        wait(df, 2, 1)
        wait(df, 2, 2)
    yield


Z_ORDER = (4, 3, 5, 2, 6, 1, 7)
SENDS = ((2, 2), (2, 1), (2, 3), (2, 0), (1, 2), (1, 1), (1, 3), (1, 0), (3, 2), (3, 1), (3, 3), (3, 0), (0, 2), (0, 1), (0, 3))
WAVES = (2, 3, 1, 0)


def mesh_kernel(*refs):
    small, (state, r_hbm, ot_hbm, gt_hbm, ut_hbm, dn_hbm, gain_hbm, bg_hbm, eg_hbm, eu_hbm, ed_hbm) = refs[:SMALL], refs[SMALL : SMALL + 11]
    new_state, out_ref = refs[SMALL + 11 : SMALL + 13]
    refs = refs[SMALL + 13 :]
    px, pz, pb, pdt, tx, tb, wx, wb, dtb, dlg, gg, ids, ew, gw = refs[:SMALL]
    (route, grid, xs_s, in_s, rd_s, de_s, rdo, disp, c_hi, c_lo, r_ref, gain, bgate,
     wbuf, obuf, ybuf, rbuf, mown, msend, mrecv, nbuf, rn, normed, dsend, drecv, xsend, xfull, emine, esend, erecv,
     csend, cbuf, tot, zsend, zrecv, fin, eg, eu, ed,
     ssem, wsem, gsem, zsem, asem, tsem, nsem, fsem, rsem, lsem, msem, isem) = refs[SMALL:]
    z, y, x, t = (lax.axis_index(a) for a in EP_TP)
    coords = {"x": x, "y": y}
    q = y * 4 + x
    other = 1 - t
    sends = [(lax.rem(y + dy, 4), lax.rem(x + dx, 4)) for dy, dx in SENDS]
    waves = [[(lax.rem(y + dy, 4), lax.rem(x + dx, 4), dy == 0 and dx == 0) for dx in (2, 3, 1, 0)] for dy in WAVES]
    zs = [lax.rem(z + d, 8) for d in Z_ORDER]

    barrier = pltpu.get_barrier_semaphore()
    for zz in zs:
        pl.semaphore_signal(barrier, inc=1, device_id={"z": zz}, device_id_type=MESH)
    for yy, xx in sends:
        pl.semaphore_signal(barrier, inc=1, device_id={"y": yy, "x": xx}, device_id_type=MESH)
    pl.semaphore_signal(barrier, inc=1, device_id={"tp": other}, device_id_type=MESH)
    for zz in zs:
        pl.semaphore_signal(barrier, inc=1, device_id={"z": zz, "tp": other}, device_id_type=MESH)

    def block(ref, half, j):
        return ref.at[:, pl.ds(half * 8, 8), pl.ds(j * WIDE, WIDE)]

    def in_copy(half, j):
        return pltpu.make_async_copy(block(state, half, j), block(new_state, half, j), isem.at[half, j])

    first = [pltpu.make_async_copy(src, dst, msem.at[i]) for i, (src, dst) in enumerate(zip(small, refs[:SMALL]))]
    for load in first[:EARLY]:
        load.start()
    for half in range(2):
        for j in range(CHUNKS):
            in_copy(half, j).start()
    pairs = ((ot_hbm, obuf.at[q]), (gt_hbm, wbuf.at[q, 0]), (ut_hbm, wbuf.at[q, 1]), (dn_hbm, wbuf.at[q, 2]), (r_hbm, r_ref),
             (gain_hbm, gain), (bg_hbm, bgate), (eg_hbm.at[0], eg), (eu_hbm.at[0], eu), (ed_hbm.at[0], ed))
    loads = [pltpu.make_async_copy(src, dst, lsem.at[i]) for i, (src, dst) in enumerate(pairs)]
    grid[...] = ((iota((128, WIDE), 0) % 64) == (iota((128, WIDE), 1) // 64)).astype(BF16)
    for load in first[:EARLY]:
        load.wait()
    for load in first[EARLY:] + loads[:5]:
        load.start()

    conv_x = px[...].astype(F32) * wx[3:4, :].astype(F32)
    for w in range(3):
        conv_x = conv_x + tx[w].astype(F32) * wx[w : w + 1, :].astype(F32)
    conv_x = silu(conv_x)
    conv_bc = pb[...].astype(F32) * wb[3:4].astype(F32)
    for w in range(3):
        conv_bc = conv_bc + tb[:, w].astype(F32) * wb[w : w + 1].astype(F32)
    conv_bc = silu(conv_bc)
    top = iota((16, 2, 256), 1) == 0
    inputs = jnp.sum(jnp.where(top, conv_bc, 0.0), axis=1)
    reads = jnp.sum(jnp.where(top, 0.0, conv_bc), axis=1)
    pre = pdt[...].astype(F32) + dtb[...]
    step = jnp.maximum(pre, 0.0) + jnp.log1p(jnp.exp(-jnp.abs(pre)))
    decay = jnp.exp(-step * jnp.exp(dlg[...]))
    for half in range(2):
        x_rows = spread(conv_x[:, half * 512 : (half + 1) * 512]) * column(step, half)
        high, low = split(x_rows)
        xs_s[half] = jnp.where(iota((128, 128), 1) < 64, high.astype(F32), low.astype(F32))
        in_s[half] = spread(inputs[:, half * 128 : (half + 1) * 128])
        rd_s[half] = spread(reads[:, half * 128 : (half + 1) * 128])
        de_s[half] = jnp.broadcast_to(column(decay, half), (128, 128))

    def advance_state(half, low, high):
        lanes = WIDE // 64
        for j in range(low, high):
            in_copy(half, j).wait()
            here = (slice(None), slice(half * 8, half * 8 + 8), slice(j * WIDE, (j + 1) * WIDE))
            shifted = xs_s[half] if j == 0 else pltpu.roll(xs_s[half], 128 - j * lanes, 1)
            fresh = dot(shifted.astype(BF16), grid[...])
            new = jnp.tile(de_s[half], (1, WIDE // 128)) * new_state[here].reshape(128, WIDE) + fresh * jnp.tile(in_s[half], (1, WIDE // 128))
            new_state[here] = new.reshape(16, 8, WIDE)
            part = dot_t((new * jnp.tile(rd_s[half], (1, WIDE // 128))).astype(BF16), grid[...])
            rdo[half] = part if j == 0 else rdo[half] + pltpu.roll(part, j * lanes, 1)

    def finish_state(half):
        keep = (iota((8, 512), 1) // 64) == iota((8, 512), 0)
        wide = jnp.tile(rdo[half], (1, 4)).reshape(16, 8, 512)
        read = jnp.sum(jnp.where(keep[None], wide, 0.0), axis=1)
        gated = read * silu(pz[:, half * 512 : (half + 1) * 512].astype(F32))
        for g in range(2):
            lanes = slice(half * 512 + g * 256, half * 512 + (g + 1) * 256)
            part = gated[:, g * 256 : (g + 1) * 256]
            scale = lax.rsqrt(jnp.mean(part * part, axis=-1, keepdims=True) + EPSILON)
            ybuf[z, :, lanes] = (part * scale * gg[:, lanes]).astype(BF16)

    copies = Copies(ssem)

    def send_y(half):
        ref = ybuf.at[z, :, half * 512 : (half + 1) * 512]
        for zz in zs:
            copies(ref, ref, zsem.at[half, z], z=zz)

    og = [plane_gather(copies, obuf, g * 512, 512, g, gsem, coords) for g in range(2)]
    wg = [plane_gather(copies, wbuf, g * 1024, 1024, g, wsem, coords) for g in range(2)]

    def advance(gens):
        for gen in gens:
            next(gen)

    advance_state(0, 0, CHUNKS)
    finish_state(0)
    for load in loads[:5]:
        load.wait()
    pl.semaphore_wait(barrier, 2 * len(zs) + len(sends) + 1)
    send_y(0)
    advance(og)
    for zz in zs:
        copies(r_ref.at[:, pl.ds(pl.multiple_of(zz * 256 + t * 128, 128), 128)], rbuf.at[z], zsem.at[2, z], z=zz)
    for load in loads[5:]:
        load.start()
    advance(wg)
    rbuf[z] = r_ref[:, pl.ds(pl.multiple_of(z * 256 + t * 128, 128), 128)]
    advance_state(1, 0, CHUNKS)
    finish_state(1)
    send_y(1)
    advance(og)
    advance(og)
    for load in first[EARLY:]:
        load.wait()
    route[...] = jnp.zeros_like(route)
    route[0:6, :] = ids[...].astype(F32)
    route[8:14, :] = ew[...]
    route[16:20, :] = gw[...]
    row, tok = iota((2048, 128), 0), iota((2048, 128), 1)
    take = (row == (tok // 16) * 256 + q * 16 + tok % 16).astype(BF16)
    high, rest = split(route[...])
    mine = dot(high, take) + dot(rest, take)
    own = iota((16, 128), 0) + z * 16
    hit = jnp.zeros((16, 128), F32)
    weight = jnp.zeros((16, 128), F32)
    for k in range(6):
        same = mine[k : k + 1, :].astype(I32) == own
        hit = hit + same.astype(F32)
        weight = weight + jnp.where(same, mine[8 + k : 9 + k, :], 0.0)
    coarse = jnp.sum(jnp.where(iota((8, 128), 0) == z // 2, mine[16:24, :], 0.0), axis=0, keepdims=True)
    weight = weight * coarse
    a, b = iota((128, 128), 0), iota((128, 128), 1)
    before = ((a // 16 == b // 16) & (a < b)).astype(BF16)
    rank = dot(hit.astype(BF16), before)
    slot, tok3 = iota((16, 16, 128), 1), iota((16, 16, 128), 2)
    chosen = (
        (hit[:, None, :] > 0.5)
        & (rank[:, None, :] == (slot % 2).astype(F32))
        & (slot // 2 == tok3 // 16)
    )
    disp[...] = jnp.where(chosen, 1.0, 0.0).reshape(256, 128).astype(BF16)
    comb = jnp.where(chosen, jnp.broadcast_to(weight[:, None, :], (16, 16, 128)), 0.0).reshape(256, 128)
    comb = jnp.concatenate([comb[:128].T, comb[128:].T], axis=1)
    high, low = split(comb)
    c_hi[...] = high
    c_lo[...] = low

    advance(og)
    advance(og)
    advance(wg)
    advance(wg)
    advance(og)
    for half in range(2):
        for zz in zs[::-1]:
            copies.arrived(ybuf.at[zz, :, half * 512 : (half + 1) * 512], zsem.at[half, zz], z=zz)

    rows = ybuf[...].reshape(128, 1024)
    msend[...] = dot_t(rows, obuf[pl.ds(other * 8, 8)].reshape(128, 1024)).astype(BF16)
    copies(msend, mrecv, tsem.at[0], tp=other)
    mown[...] = dot_t(rows, obuf[pl.ds(t * 8, 8)].reshape(128, 1024))
    for zz in zs:
        copies.arrived(rbuf.at[zz], zsem.at[2, zz], z=zz)
    copies.arrived(mrecv, tsem.at[0], tp=other)
    mixed = mown[...] + mrecv[...].astype(F32)
    nbuf[z, t] = (rbuf[...].reshape(128, 128).astype(F32) + mixed).astype(BF16)
    for zz in zs:
        copies(nbuf.at[z, t], nbuf.at[z, t], zsem.at[3, z], z=zz)
    copies(nbuf.at[z, t], nbuf.at[z, t], nsem.at[z], tp=other)
    advance(wg)
    for i, zz in enumerate(zs):
        if i == 4:
            advance(wg)
        copies.arrived(nbuf.at[zz, t], zsem.at[3, zz], z=zz)
        copies(nbuf.at[zz, t], nbuf.at[zz, t], nsem.at[zz], tp=other)
    for load in loads[5:]:
        load.wait()
    for zz in [z] + zs:
        copies.arrived(nbuf.at[zz, other], nsem.at[zz], tp=other)

    for j in range(16):
        rn[:, j * 128 : (j + 1) * 128] = nbuf[j // 2, j % 2]
    wide = rn[...].astype(F32)
    scale = lax.rsqrt(jnp.mean(wide * wide, axis=-1, keepdims=True) + EPSILON)
    normed[...] = (wide * scale * gain[...]).astype(BF16)
    near = pl.ds(pl.multiple_of(t * 1024, 1024), 1024)
    far = pl.ds(pl.multiple_of(other * 1024, 1024), 1024)

    xsend[...] = dot(disp[...], normed[:, near]).astype(BF16).reshape(16, 16, 1024)
    for yy, xx in sends:
        copies(xsend.at[yy * 4 + xx], xfull.at[t, q], asem.at[0, q], y=yy, x=xx)
    xfull[t, q] = xsend[q]
    copies(xsend.at[q], xfull.at[t, q], fsem.at[q], tp=other)

    advance(wg)
    tokens = normed[...]
    vector = jnp.concatenate([bgate[j : j + 1, :].astype(F32) for j in range(16)], axis=1)
    score = jnp.sum(tokens.astype(F32) * vector, axis=-1, keepdims=True)
    gate = dot_t(tokens, wbuf[:, 0].reshape(256, 2048))
    lin = dot_t(tokens, wbuf[:, 1].reshape(256, 2048))
    hidden = (silu(gate) * lin / (1.0 + jnp.exp(-score))).astype(BF16)
    dsend[...] = dot(hidden, wbuf[:, 2, :, far].reshape(256, 1024)).astype(BF16)
    copies(dsend, drecv, tsem.at[1], tp=other)
    tot[...] = dot(hidden, wbuf[:, 2, :, near].reshape(256, 1024)).reshape(8, 16, 1024)

    def receive(w):
        for yy, xx, self in waves[w]:
            if not self:
                qq = yy * 4 + xx
                copies.arrived(xfull.at[t, qq], asem.at[0, qq], y=yy, x=xx)
                copies(xfull.at[t, qq], xfull.at[t, qq], fsem.at[qq], tp=other)

    def compute(w):
        places = [yy * 4 + xx for yy, xx, _ in waves[w]]
        for qq in places:
            copies.arrived(xfull.at[other, qq], fsem.at[qq], tp=other)
        left = jnp.concatenate([xfull[0, qq] for qq in places], axis=0)
        right = jnp.concatenate([xfull[1, qq] for qq in places], axis=0)
        gate = dot(left, eg[0:1024, :]) + dot(right, eg[1024:2048, :])
        lin = dot(left, eu[0:1024, :]) + dot(right, eu[1024:2048, :])
        hidden = (silu(gate) * lin).astype(BF16)
        esend[w] = dot(hidden, ed[:, far]).astype(BF16)
        copies(esend.at[w], erecv.at[w], tsem.at[4 + w], tp=other)
        emine[w] = dot(hidden, ed[:, near])

    def send_back(c, yy, xx):
        lanes = pl.ds(c * 512, 512)
        copies(csend.at[yy * 4 + xx, :, lanes], cbuf.at[q, :, lanes], asem.at[1 + c, q], y=yy, x=xx)

    def give_back(w):
        copies.arrived(erecv.at[w], tsem.at[4 + w], tp=other)
        done = (emine[w] + erecv[w].astype(F32)).astype(BF16)
        for i, (yy, xx, self) in enumerate(waves[w]):
            qq = yy * 4 + xx
            if self:
                cbuf[q] = done[i * 16 : (i + 1) * 16]
            else:
                csend[qq] = done[i * 16 : (i + 1) * 16]
                send_back(0, yy, xx)

    receive(0)
    receive(1)
    compute(0)
    receive(2)
    compute(1)
    give_back(0)
    receive(3)
    compute(2)
    give_back(1)
    compute(3)
    give_back(2)
    give_back(3)
    for w in range(4):
        for yy, xx, self in waves[w]:
            if not self:
                send_back(1, yy, xx)
    copies.arrived(drecv, tsem.at[1], tp=other)
    fin[...] = rn[pl.ds(pl.multiple_of(z * 16, 16), 16), :].astype(F32)
    for c in range(2):
        lanes = slice(c * 512, (c + 1) * 512)
        base = tot[:, :, lanes].reshape(128, 512) + drecv[:, lanes].astype(F32)
        for w in range(4):
            for yy, xx, self in waves[(w + 1) % 4 if w < 3 else 0]:
                if not self:
                    qq = yy * 4 + xx
                    copies.arrived(cbuf.at[qq, :, lanes], asem.at[1 + c, qq], y=yy, x=xx)
        back = cbuf[:, :, lanes].reshape(256, 512)
        total = base + dot(c_hi[...], back) + dot(c_lo[...], back)
        tot[:, :, lanes] = total.reshape(8, 16, 512)
        zsend[c] = total.reshape(8, 2, 8, 512).astype(BF16)
        for zz in zs:
            for tt in (t, other):
                copies(zsend.at[c, zz, tt], zrecv.at[c, z, t], rsem.at[c, z, t], z=zz, tp=tt)
        copies(zsend.at[c, z, other], zrecv.at[c, z, t], rsem.at[c, z, t], tp=other)
    for c in range(2):
        for side in (t, other):
            lanes = pl.ds(pl.multiple_of(side * 1024 + c * 512, 512), 512)
            final = fin[pl.ds(pl.multiple_of(t * 8, 8), 8), lanes]
            if side is t:
                final = final + tot[z, pl.ds(pl.multiple_of(t * 8, 8), 8), c * 512 : (c + 1) * 512]
            for zz in zs if side is t else [z] + zs:
                copies.arrived(zrecv.at[c, zz, side], rsem.at[c, zz, side], tp=other)
                final = final + zrecv[c, zz, side].astype(F32)
            out_ref[:, lanes] = final.astype(BF16)
    copies.drain()


def shards(resid, proj_x, proj_z, proj_bc, proj_dt, tail_x, tail_bc, taps_x, taps_bc, ssm_state, dt_bias, decay_log,
           group_gain, out_proj, ffn_gain, dense_gate, dense_up, dense_down, branch_gate, group_weights, expert_ids,
           expert_weights, exp_gate, exp_up, exp_down):
    small = (proj_x, proj_z, proj_bc, proj_dt, tail_x.transpose(1, 0, 2), tail_bc, taps_x, taps_bc, dt_bias.reshape(1, 16),
             decay_log.reshape(1, 16), group_gain.reshape(1, 1024), expert_ids.T, expert_weights.T, group_weights.T)
    vm = pl.BlockSpec(memory_space=VMEM)
    hbm = pl.BlockSpec(memory_space=pltpu.MemorySpace.HBM)
    scratch = [pltpu.VMEM(a.shape, a.dtype) for a in small]
    for shape, dtype in (
        ((32, 2048), F32), ((128, WIDE), BF16), ((2, 128, 128), F32), ((2, 128, 128), F32), ((2, 128, 128), F32),
        ((2, 128, 128), F32), ((2, 128, 128), F32), ((256, 128), BF16), ((128, 256), BF16), ((128, 256), BF16),
        ((16, 2048), BF16), ((1, 2048), F32), ((16, 128), BF16),
        ((16, 3, 16, 2048), BF16), ((16, 16, 1024), BF16), ((8, 16, 1024), BF16), ((8, 16, 128), BF16),
        ((128, 128), F32), ((128, 128), BF16), ((128, 128), BF16), ((8, 2, 128, 128), BF16), ((128, 2048), BF16),
        ((128, 2048), BF16), ((128, 1024), BF16), ((128, 1024), BF16), ((16, 16, 1024), BF16), ((2, 16, 16, 1024), BF16),
        ((4, 64, 1024), F32), ((4, 64, 1024), BF16), ((4, 64, 1024), BF16), ((16, 16, 1024), BF16), ((16, 16, 1024), BF16),
        ((8, 16, 1024), F32), ((2, 8, 2, 8, 512), BF16), ((2, 8, 2, 8, 512), BF16), ((16, 2048), F32),
        ((2048, 256), BF16), ((2048, 256), BF16), ((256, 2048), BF16),
    ):
        scratch.append(pltpu.VMEM(shape, dtype))
    for shape in ((224,), (2, 16, 2), (2, 16, 2), (4, 8), (3, 16), (8,), (8,), (16,), (2, 8, 2), (10,), (SMALL,), (2, CHUNKS)):
        scratch.append(pltpu.SemaphoreType.DMA(shape))
    new_state, out = pl.pallas_call(
        mesh_kernel,
        out_shape=(VMEM((16, 16, 4096), F32), VMEM((8, 2048), BF16)),
        in_specs=[hbm] * (SMALL + 11),
        out_specs=(vm, vm),
        scratch_shapes=scratch,
        compiler_params=pltpu.CompilerParams(collective_id=0, has_side_effects=True, vmem_limit_bytes=67_043_328 - (4200 << 10)),
        name="mesh",
    )(*small, ssm_state, resid, out_proj.T, dense_gate.T, dense_up.T, dense_down, ffn_gain.reshape(1, 2048),
      branch_gate.reshape(16, 128), exp_gate, exp_up, exp_down)
    return (out, new_state)


def solution(mesh):
    finer = Mesh(mesh.devices.reshape(NZ, NY, NX, mesh.shape["tp"]), EP_TP)
    in_specs = (
        P(EP, None), P(EP, "tp"), P(EP, "tp"), P(EP, None, "tp"), P(EP, "tp"), P(EP, None, "tp"), P(EP, None, None, "tp"),
        P(None, "tp"), P(None, None, "tp"), P(EP, "tp", None), P("tp"), P("tp"), P("tp"), P("tp", EP), P(),
        P(None, EP_TP), P(None, EP_TP), P(EP_TP, None), P(), P(), P(), P(), P(EP, None, "tp"), P(EP, None, "tp"),
        P(EP, "tp", None),
    )
    out_specs = (P(EP_TP, None), P(EP, "tp", None))
    return jax.shard_map(shards, mesh=finer, in_specs=in_specs, out_specs=out_specs, check_vma=False)
```

time: 89.9 us -> 71.1 us (0.79)
  local copies, waits for them, and re-layouts: 11.8 us -> 2.63 us
  Pallas kernels: 74.9 us -> 67.8 us
  other arithmetic: 1.7 us -> 0 us
    unnamed x43 -> x2, local copies, waits for them, and re-layouts: 11.1 us -> 2.63 us
    pallas_call x2 -> x1, Pallas kernels: 74.9 us -> 67.8 us  [shards(): pl.pallas_call(mesh_kernel, out_shape=(VMEM((16, 16, 4096), F32), VMEM((8...]
    reduce_sum x1 -> x0, other arithmetic: 0.93 us -> none  [shards(): jnp.sum(window * taps_bc.astype(F32)[None], axis=1)]
where the time goes in v2:
time: 71.1 us; the launch traced here: 71 us
  Pallas kernels  67.8 us (95%)
  local copies, waits for them, and re-layouts  2.63 us (4%)
    pallas_call x1, Pallas kernels, shards(): pl.pallas_call(mesh_kernel, out_shape=(VMEM((16, 16, 4096), F32), VMEM((8...  67.8 us
    unnamed x2, local copies, waits for them, and re-layouts  2.63 us

profile of v2, /device:TPU:1, one launch (start us, length us, event | category | flops | bytes accessed | tf_op | source)
XLA Modules:
  0.0 71.0 jit_solution(12497341990845653880)
XLA Ops:
  0.6 67.8 %mesh.1 = (f32[16,16,4096]{2,1,0:T(8,128)S(1)}, bf16[8,2048]{1,0:T(8,128)(2,1)S(1)}) custom-call(bf16[16,1024]{1,0:T(8,128)(2,1)} %refs_0_.1, bf16[16,1024]{1,0:T(8,128)(2,1)} %refs_1_.1, bf16[16,2,256]{2,1,0:T(2,128)(2,1)} %refs_2_.1, bf16[16,16]{1,0:T(8,128)(2,1)} %refs_3_.1, bf16[3,16,1024]{2,1,0:T(8,128)(2,1)} %bitcast.12, ...), custom_call_target="tpu_custom_call" | custom-call | tf_op jit(solution)/shard_map/mesh/pallas_call | solution.py:465
  68.4 0.6 copy.29
  69.0 2.0 %copy.30 = f32[16,16,4096]{2,1,0:T(8,128)} copy(f32[16,16,4096]{2,1,0:T(8,128)S(1)} %get-tuple-element.7) | data formatting | bytes 8388608

commit v3 on v2

--- a/solution.py
+++ b/solution.py
@@ -18,6 +18,8 @@
 CHUNKS = 4
 WIDE = 4096 // CHUNKS
 EARLY = 11
+PARTS = 2
+PART = 1024 // PARTS
 SMALL = 14
 
 
@@ -122,6 +124,7 @@
     wait(2, 0, 2)
     for move in (1, -1):
         send(2, 0, 0, sa, move)
+    yield
     for df in (-1, 1):
         for ds, part in turns:
             wait(df, ds, 0)
@@ -139,7 +142,7 @@
 
 Z_ORDER = (4, 3, 5, 2, 6, 1, 7)
 SENDS = ((2, 2), (2, 1), (2, 3), (2, 0), (1, 2), (1, 1), (1, 3), (1, 0), (3, 2), (3, 1), (3, 3), (3, 0), (0, 2), (0, 1), (0, 3))
-WAVES = (2, 3, 1, 0)
+WAVES = ((2, 3), (1, 0))
 
 
 def mesh_kernel(*refs):
@@ -156,7 +159,7 @@
     q = y * 4 + x
     other = 1 - t
     sends = [(lax.rem(y + dy, 4), lax.rem(x + dx, 4)) for dy, dx in SENDS]
-    waves = [[(lax.rem(y + dy, 4), lax.rem(x + dx, 4), dy == 0 and dx == 0) for dx in (2, 3, 1, 0)] for dy in WAVES]
+    waves = [[(lax.rem(y + dy, 4), lax.rem(x + dx, 4), dy == 0 and dx == 0) for dy in wave for dx in (2, 3, 1, 0)] for wave in WAVES]
     zs = [lax.rem(z + d, 8) for d in Z_ORDER]
 
     barrier = pltpu.get_barrier_semaphore()
@@ -177,16 +180,17 @@
     first = [pltpu.make_async_copy(src, dst, msem.at[i]) for i, (src, dst) in enumerate(zip(small, refs[:SMALL]))]
     for load in first[:EARLY]:
         load.start()
-    for half in range(2):
-        for j in range(CHUNKS):
-            in_copy(half, j).start()
-    pairs = ((ot_hbm, obuf.at[q]), (gt_hbm, wbuf.at[q, 0]), (ut_hbm, wbuf.at[q, 1]), (dn_hbm, wbuf.at[q, 2]), (r_hbm, r_ref),
+    for j in range(CHUNKS):
+        in_copy(0, j).start()
+    pairs = ((ot_hbm, obuf.at[y, x]), (gt_hbm, wbuf.at[q, 0]), (ut_hbm, wbuf.at[q, 1]), (dn_hbm, wbuf.at[q, 2]), (r_hbm, r_ref),
              (gain_hbm, gain), (bg_hbm, bgate), (eg_hbm.at[0], eg), (eu_hbm.at[0], eu), (ed_hbm.at[0], ed))
     loads = [pltpu.make_async_copy(src, dst, lsem.at[i]) for i, (src, dst) in enumerate(pairs)]
     grid[...] = ((iota((128, WIDE), 0) % 64) == (iota((128, WIDE), 1) // 64)).astype(BF16)
     for load in first[:EARLY]:
         load.wait()
-    for load in first[EARLY:] + loads[:5]:
+    for j in range(CHUNKS):
+        in_copy(1, j).start()
+    for load in loads[:5] + first[EARLY:]:
         load.start()
 
     conv_x = px[...].astype(F32) * wx[3:4, :].astype(F32)
@@ -215,13 +219,17 @@
         lanes = WIDE // 64
         for j in range(low, high):
             in_copy(half, j).wait()
+        total = None
+        for j in range(low, high):
             here = (slice(None), slice(half * 8, half * 8 + 8), slice(j * WIDE, (j + 1) * WIDE))
             shifted = xs_s[half] if j == 0 else pltpu.roll(xs_s[half], 128 - j * lanes, 1)
             fresh = dot(shifted.astype(BF16), grid[...])
             new = jnp.tile(de_s[half], (1, WIDE // 128)) * new_state[here].reshape(128, WIDE) + fresh * jnp.tile(in_s[half], (1, WIDE // 128))
             new_state[here] = new.reshape(16, 8, WIDE)
             part = dot_t((new * jnp.tile(rd_s[half], (1, WIDE // 128))).astype(BF16), grid[...])
-            rdo[half] = part if j == 0 else rdo[half] + pltpu.roll(part, j * lanes, 1)
+            part = part if j == 0 else pltpu.roll(part, j * lanes, 1)
+            total = part if total is None else total + part
+        rdo[half] = total if low == 0 else rdo[half] + total
 
     def finish_state(half):
         keep = (iota((8, 512), 1) // 64) == iota((8, 512), 0)
@@ -241,7 +249,6 @@
         for zz in zs:
             copies(ref, ref, zsem.at[half, z], z=zz)
 
-    og = [plane_gather(copies, obuf, g * 512, 512, g, gsem, coords) for g in range(2)]
     wg = [plane_gather(copies, wbuf, g * 1024, 1024, g, wsem, coords) for g in range(2)]
 
     def advance(gens):
@@ -254,18 +261,17 @@
         load.wait()
     pl.semaphore_wait(barrier, 2 * len(zs) + len(sends) + 1)
     send_y(0)
-    advance(og)
+    for yy, xx in sends:
+        copies(obuf.at[y, x], obuf.at[y, x], gsem.at[q], y=yy, x=xx)
     for zz in zs:
         copies(r_ref.at[:, pl.ds(pl.multiple_of(zz * 256 + t * 128, 128), 128)], rbuf.at[z], zsem.at[2, z], z=zz)
+    advance(wg)
     for load in loads[5:]:
         load.start()
-    advance(wg)
     rbuf[z] = r_ref[:, pl.ds(pl.multiple_of(z * 256 + t * 128, 128), 128)]
     advance_state(1, 0, CHUNKS)
     finish_state(1)
     send_y(1)
-    advance(og)
-    advance(og)
     for load in first[EARLY:]:
         load.wait()
     route[...] = jnp.zeros_like(route)
@@ -276,11 +282,11 @@
     take = (row == (tok // 16) * 256 + q * 16 + tok % 16).astype(BF16)
     high, rest = split(route[...])
     mine = dot(high, take) + dot(rest, take)
-    own = iota((16, 128), 0) + z * 16
+    expert = iota((16, 128), 0) + z * 16
     hit = jnp.zeros((16, 128), F32)
     weight = jnp.zeros((16, 128), F32)
     for k in range(6):
-        same = mine[k : k + 1, :].astype(I32) == own
+        same = mine[k : k + 1, :].astype(I32) == expert
         hit = hit + same.astype(F32)
         weight = weight + jnp.where(same, mine[8 + k : 9 + k, :], 0.0)
     coarse = jnp.sum(jnp.where(iota((8, 128), 0) == z // 2, mine[16:24, :], 0.0), axis=0, keepdims=True)
@@ -301,19 +307,16 @@
     c_hi[...] = high
     c_lo[...] = low
 
-    advance(og)
-    advance(og)
-    advance(wg)
-    advance(wg)
-    advance(og)
     for half in range(2):
         for zz in zs[::-1]:
             copies.arrived(ybuf.at[zz, :, half * 512 : (half + 1) * 512], zsem.at[half, zz], z=zz)
 
+    for yy, xx in sends:
+        copies.arrived(obuf.at[yy, xx], gsem.at[yy * 4 + xx], y=yy, x=xx)
     rows = ybuf[...].reshape(128, 1024)
-    msend[...] = dot_t(rows, obuf[pl.ds(other * 8, 8)].reshape(128, 1024)).astype(BF16)
+    msend[...] = dot_t(rows, obuf[pl.ds(other * 2, 2)].reshape(128, 1024)).astype(BF16)
     copies(msend, mrecv, tsem.at[0], tp=other)
-    mown[...] = dot_t(rows, obuf[pl.ds(t * 8, 8)].reshape(128, 1024))
+    mown[...] = dot_t(rows, obuf[pl.ds(t * 2, 2)].reshape(128, 1024))
     for zz in zs:
         copies.arrived(rbuf.at[zz], zsem.at[2, zz], z=zz)
     copies.arrived(mrecv, tsem.at[0], tp=other)
@@ -323,9 +326,9 @@
         copies(nbuf.at[z, t], nbuf.at[z, t], zsem.at[3, z], z=zz)
     copies(nbuf.at[z, t], nbuf.at[z, t], nsem.at[z], tp=other)
     advance(wg)
+    advance(wg)
+    advance(wg)
     for i, zz in enumerate(zs):
-        if i == 4:
-            advance(wg)
         copies.arrived(nbuf.at[zz, t], zsem.at[3, zz], z=zz)
         copies(nbuf.at[zz, t], nbuf.at[zz, t], nsem.at[zz], tp=other)
     for load in loads[5:]:
@@ -348,15 +351,7 @@
     copies(xsend.at[q], xfull.at[t, q], fsem.at[q], tp=other)
 
     advance(wg)
-    tokens = normed[...]
-    vector = jnp.concatenate([bgate[j : j + 1, :].astype(F32) for j in range(16)], axis=1)
-    score = jnp.sum(tokens.astype(F32) * vector, axis=-1, keepdims=True)
-    gate = dot_t(tokens, wbuf[:, 0].reshape(256, 2048))
-    lin = dot_t(tokens, wbuf[:, 1].reshape(256, 2048))
-    hidden = (silu(gate) * lin / (1.0 + jnp.exp(-score))).astype(BF16)
-    dsend[...] = dot(hidden, wbuf[:, 2, :, far].reshape(256, 1024)).astype(BF16)
-    copies(dsend, drecv, tsem.at[1], tp=other)
-    tot[...] = dot(hidden, wbuf[:, 2, :, near].reshape(256, 1024)).reshape(8, 16, 1024)
+    advance(wg)
 
     def receive(w):
         for yy, xx, self in waves[w]:
@@ -379,7 +374,7 @@
         emine[w] = dot(hidden, ed[:, near])
 
     def send_back(c, yy, xx):
-        lanes = pl.ds(c * 512, 512)
+        lanes = pl.ds(c * PART, PART)
         copies(csend.at[yy * 4 + xx, :, lanes], cbuf.at[q, :, lanes], asem.at[1 + c, q], y=yy, x=xx)
 
     def give_back(w):
@@ -396,43 +391,49 @@
     receive(0)
     receive(1)
     compute(0)
-    receive(2)
     compute(1)
     give_back(0)
-    receive(3)
-    compute(2)
     give_back(1)
-    compute(3)
-    give_back(2)
-    give_back(3)
-    for w in range(4):
-        for yy, xx, self in waves[w]:
-            if not self:
-                send_back(1, yy, xx)
+    for c in range(1, PARTS):
+        for wave in waves:
+            for yy, xx, self in wave:
+                if not self:
+                    send_back(c, yy, xx)
+    advance(wg)
+    tokens = normed[...]
+    vector = jnp.concatenate([bgate[j : j + 1, :].astype(F32) for j in range(16)], axis=1)
+    score = jnp.sum(tokens.astype(F32) * vector, axis=-1, keepdims=True)
+    gate = dot_t(tokens, wbuf[:, 0].reshape(256, 2048))
+    lin = dot_t(tokens, wbuf[:, 1].reshape(256, 2048))
+    hidden = (silu(gate) * lin / (1.0 + jnp.exp(-score))).astype(BF16)
+    dsend[...] = dot(hidden, wbuf[:, 2, :, far].reshape(256, 1024)).astype(BF16)
+    copies(dsend, drecv, tsem.at[1], tp=other)
+    tot[...] = dot(hidden, wbuf[:, 2, :, near].reshape(256, 1024)).reshape(8, 16, 1024)
+
     copies.arrived(drecv, tsem.at[1], tp=other)
     fin[...] = rn[pl.ds(pl.multiple_of(z * 16, 16), 16), :].astype(F32)
-    for c in range(2):
-        lanes = slice(c * 512, (c + 1) * 512)
-        base = tot[:, :, lanes].reshape(128, 512) + drecv[:, lanes].astype(F32)
-        for w in range(4):
-            for yy, xx, self in waves[(w + 1) % 4 if w < 3 else 0]:
+    for c in range(PARTS):
+        lanes = slice(c * PART, (c + 1) * PART)
+        base = tot[:, :, lanes].reshape(128, PART) + drecv[:, lanes].astype(F32)
+        for wave in waves:
+            for yy, xx, self in wave:
                 if not self:
                     qq = yy * 4 + xx
                     copies.arrived(cbuf.at[qq, :, lanes], asem.at[1 + c, qq], y=yy, x=xx)
-        back = cbuf[:, :, lanes].reshape(256, 512)
+        back = cbuf[:, :, lanes].reshape(256, PART)
         total = base + dot(c_hi[...], back) + dot(c_lo[...], back)
-        tot[:, :, lanes] = total.reshape(8, 16, 512)
-        zsend[c] = total.reshape(8, 2, 8, 512).astype(BF16)
+        tot[:, :, lanes] = total.reshape(8, 16, PART)
+        zsend[c] = total.reshape(8, 2, 8, PART).astype(BF16)
         for zz in zs:
             for tt in (t, other):
                 copies(zsend.at[c, zz, tt], zrecv.at[c, z, t], rsem.at[c, z, t], z=zz, tp=tt)
         copies(zsend.at[c, z, other], zrecv.at[c, z, t], rsem.at[c, z, t], tp=other)
-    for c in range(2):
+    for c in range(PARTS):
         for side in (t, other):
-            lanes = pl.ds(pl.multiple_of(side * 1024 + c * 512, 512), 512)
+            lanes = pl.ds(pl.multiple_of(side * 1024 + c * PART, PART), PART)
             final = fin[pl.ds(pl.multiple_of(t * 8, 8), 8), lanes]
             if side is t:
-                final = final + tot[z, pl.ds(pl.multiple_of(t * 8, 8), 8), c * 512 : (c + 1) * 512]
+                final = final + tot[z, pl.ds(pl.multiple_of(t * 8, 8), 8), c * PART : (c + 1) * PART]
             for zz in zs if side is t else [z] + zs:
                 copies.arrived(zrecv.at[c, zz, side], rsem.at[c, zz, side], tp=other)
                 final = final + zrecv[c, zz, side].astype(F32)
@@ -452,15 +453,15 @@
         ((32, 2048), F32), ((128, WIDE), BF16), ((2, 128, 128), F32), ((2, 128, 128), F32), ((2, 128, 128), F32),
         ((2, 128, 128), F32), ((2, 128, 128), F32), ((256, 128), BF16), ((128, 256), BF16), ((128, 256), BF16),
         ((16, 2048), BF16), ((1, 2048), F32), ((16, 128), BF16),
-        ((16, 3, 16, 2048), BF16), ((16, 16, 1024), BF16), ((8, 16, 1024), BF16), ((8, 16, 128), BF16),
+        ((16, 3, 16, 2048), BF16), ((4, 4, 16, 1024), BF16), ((8, 16, 1024), BF16), ((8, 16, 128), BF16),
         ((128, 128), F32), ((128, 128), BF16), ((128, 128), BF16), ((8, 2, 128, 128), BF16), ((128, 2048), BF16),
         ((128, 2048), BF16), ((128, 1024), BF16), ((128, 1024), BF16), ((16, 16, 1024), BF16), ((2, 16, 16, 1024), BF16),
-        ((4, 64, 1024), F32), ((4, 64, 1024), BF16), ((4, 64, 1024), BF16), ((16, 16, 1024), BF16), ((16, 16, 1024), BF16),
-        ((8, 16, 1024), F32), ((2, 8, 2, 8, 512), BF16), ((2, 8, 2, 8, 512), BF16), ((16, 2048), F32),
+        ((2, 128, 1024), F32), ((2, 128, 1024), BF16), ((2, 128, 1024), BF16), ((16, 16, 1024), BF16), ((16, 16, 1024), BF16),
+        ((8, 16, 1024), F32), ((PARTS, 8, 2, 8, PART), BF16), ((PARTS, 8, 2, 8, PART), BF16), ((16, 2048), F32),
         ((2048, 256), BF16), ((2048, 256), BF16), ((256, 2048), BF16),
     ):
         scratch.append(pltpu.VMEM(shape, dtype))
-    for shape in ((224,), (2, 16, 2), (2, 16, 2), (4, 8), (3, 16), (8,), (8,), (16,), (2, 8, 2), (10,), (SMALL,), (2, CHUNKS)):
+    for shape in ((160 + 45 * PARTS,), (2, 16, 2), (16,), (4, 8), (1 + PARTS, 16), (8,), (8,), (16,), (PARTS, 8, 2), (10,), (SMALL,), (2, CHUNKS)):
         scratch.append(pltpu.SemaphoreType.DMA(shape))
     new_state, out = pl.pallas_call(
         mesh_kernel,

time: 71.1 us -> 64.3 us (0.904)
  Pallas kernels: 67.8 us -> 60.9 us
    pallas_call x1, Pallas kernels: 67.8 us -> 60.9 us  [shards(): pl.pallas_call(mesh_kernel, out_shape=(VMEM((16, 16, 4096), F32), VMEM((8...]
where the time goes in v3:
time: 64.3 us; the launch traced here: 64.2 us
  Pallas kernels  60.9 us (95%)
  local copies, waits for them, and re-layouts  2.63 us (4%)
  between operations  0.65 us (1%)
    pallas_call x1, Pallas kernels, shards(): pl.pallas_call(mesh_kernel, out_shape=(VMEM((16, 16, 4096), F32), VMEM((8...  60.9 us
    unnamed x2, local copies, waits for them, and re-layouts  2.63 us

profile of v3, /device:TPU:1, one launch (start us, length us, event | category | flops | bytes accessed | tf_op | source)
XLA Modules:
  0.0 64.2 jit_solution(11040892401698770571)
XLA Ops:
  0.6 60.9 %mesh.1 = (f32[16,16,4096]{2,1,0:T(8,128)S(1)}, bf16[8,2048]{1,0:T(8,128)(2,1)S(1)}) custom-call(bf16[16,1024]{1,0:T(8,128)(2,1)} %refs_0_.1, bf16[16,1024]{1,0:T(8,128)(2,1)} %refs_1_.1, bf16[16,2,256]{2,1,0:T(2,128)(2,1)} %refs_2_.1, bf16[16,16]{1,0:T(8,128)(2,1)} %refs_3_.1, bf16[3,16,1024]{2,1,0:T(8,128)(2,1)} %bitcast.12, ...), custom_call_target="tpu_custom_call" | custom-call | tf_op jit(solution)/shard_map/mesh/pallas_call | solution.py:466
  61.5 0.6 copy.29
  62.2 2.0 %copy.30 = f32[16,16,4096]{2,1,0:T(8,128)} copy(f32[16,16,4096]{2,1,0:T(8,128)S(1)} %get-tuple-element.7) | data formatting | bytes 8388608

commit v4 on v3

--- a/solution.py
+++ b/solution.py
@@ -263,8 +263,6 @@
     send_y(0)
     for yy, xx in sends:
         copies(obuf.at[y, x], obuf.at[y, x], gsem.at[q], y=yy, x=xx)
-    for zz in zs:
-        copies(r_ref.at[:, pl.ds(pl.multiple_of(zz * 256 + t * 128, 128), 128)], rbuf.at[z], zsem.at[2, z], z=zz)
     advance(wg)
     for load in loads[5:]:
         load.start()
@@ -272,6 +270,8 @@
     advance_state(1, 0, CHUNKS)
     finish_state(1)
     send_y(1)
+    for zz in zs:
+        copies(r_ref.at[:, pl.ds(pl.multiple_of(zz * 256 + t * 128, 128), 128)], rbuf.at[z], zsem.at[2, z], z=zz)
     for load in first[EARLY:]:
         load.wait()
     route[...] = jnp.zeros_like(route)
@@ -362,12 +362,14 @@
 
     def compute(w):
         places = [yy * 4 + xx for yy, xx, _ in waves[w]]
+        mine = jnp.concatenate([xfull[t, qq] for qq in places], axis=0)
+        gate = dot(mine, eg[near, :])
+        lin = dot(mine, eu[near, :])
         for qq in places:
             copies.arrived(xfull.at[other, qq], fsem.at[qq], tp=other)
-        left = jnp.concatenate([xfull[0, qq] for qq in places], axis=0)
-        right = jnp.concatenate([xfull[1, qq] for qq in places], axis=0)
-        gate = dot(left, eg[0:1024, :]) + dot(right, eg[1024:2048, :])
-        lin = dot(left, eu[0:1024, :]) + dot(right, eu[1024:2048, :])
+        theirs = jnp.concatenate([xfull[other, qq] for qq in places], axis=0)
+        gate = gate + dot(theirs, eg[far, :])
+        lin = lin + dot(theirs, eu[far, :])
         hidden = (silu(gate) * lin).astype(BF16)
         esend[w] = dot(hidden, ed[:, far]).astype(BF16)
         copies(esend.at[w], erecv.at[w], tsem.at[4 + w], tp=other)

time: 64.3 us -> 64.5 us (level)
  no operation moved by 1% of the time
where the time goes in v4:
time: 64.5 us; the launch traced here: 64.4 us
  Pallas kernels  61.1 us (95%)
  local copies, waits for them, and re-layouts  2.63 us (4%)
  between operations  0.65 us (1%)
    pallas_call x1, Pallas kernels, shards(): pl.pallas_call(mesh_kernel, out_shape=(VMEM((16, 16, 4096), F32), VMEM((8...  61.1 us
    unnamed x2, local copies, waits for them, and re-layouts  2.63 us

profile of v4, /device:TPU:1, one launch (start us, length us, event | category | flops | bytes accessed | tf_op | source)
XLA Modules:
  0.0 64.4 jit_solution(7360286894899208331)
XLA Ops:
  0.6 61.1 %mesh.1 = (f32[16,16,4096]{2,1,0:T(8,128)S(1)}, bf16[8,2048]{1,0:T(8,128)(2,1)S(1)}) custom-call(bf16[16,1024]{1,0:T(8,128)(2,1)} %refs_0_.1, bf16[16,1024]{1,0:T(8,128)(2,1)} %refs_1_.1, bf16[16,2,256]{2,1,0:T(2,128)(2,1)} %refs_2_.1, bf16[16,16]{1,0:T(8,128)(2,1)} %refs_3_.1, bf16[3,16,1024]{2,1,0:T(8,128)(2,1)} %bitcast.12, ...), custom_call_target="tpu_custom_call" | custom-call | tf_op jit(solution)/shard_map/mesh/pallas_call | solution.py:468
  61.8 0.6 copy.29
  62.4 2.0 %copy.30 = f32[16,16,4096]{2,1,0:T(8,128)} copy(f32[16,16,4096]{2,1,0:T(8,128)S(1)} %get-tuple-element.7) | data formatting | bytes 8388608
